TPU v7x, 128 devices: a whole 4x4x4 slice. The times are simulated.
128 devices in a mesh: sp: 16 (over z, y), tp: 8 (over x, core).
Axes of the slice: x: 4, y: 4, z: 4, core: 2. Of those that a mesh axis runs over, the one named last changes fastest.
Arguments:
- query_proj: bfloat16 [16384, 2048], P('sp', 'tp'), may hold values from -6 to 6
- key_proj: bfloat16 [16384, 2048], P('sp', 'tp'), may hold values from -6 to 6
- value_proj: bfloat16 [16384, 4096], P('sp', 'tp'), may hold values from -6 to 6
- gate_proj: bfloat16 [16384, 4096], P('sp', 'tp'), may hold values from -6 to 6
- log_decay: float32 [16384, 8], P('sp', 'tp'), may hold values from -0.75 to 0, as said below
- residual: bfloat16 [16384, 2048], P('sp'), may hold values from -4 to 4
- out_weight: bfloat16 [4096, 2048], P('tp'), may hold values from -0.09375 to 0.09375
- norm_gain: float32 [2, 2048], replicated, may hold values from 0.1 to 1.9
- norm_bias: float32 [2, 2048], replicated, may hold values from -1.5 to 1.5
- up_gate: bfloat16 [2048, 5632], P('sp', 'tp'), may hold values from -0.125 to 0.125
- up_value: bfloat16 [2048, 5632], P('sp', 'tp'), may hold values from -0.125 to 0.125
- conv_weight: float32 [2, 3, 5632], P(None, None, 'tp'), may hold values from -3 to 3
- conv_bias: float32 [2, 5632], P(None, 'tp'), may hold values from -1.5 to 1.5
- down_weight: bfloat16 [5632, 2048], P('tp', 'sp'), may hold values from -0.078125 to 0.078125
Outputs:
- layer_output: bfloat16 [16384, 2048], P(('sp', 'tp'))
Inputs may be any that keep to these rules, and one draw needn't show every extreme that they name: `log_decay`: all entries are negative.
All inputs are finite; a program needn't handle non-finite values.
Results may differ from a plain program's by a relative error of at most 0.023.
Values may be sent and summed in bfloat16 or wider, within the bound.
A program may use at most 128 MiB of HBM per device.

v0:
```python
import jax
import jax.numpy as jnp
from jax import lax
from jax.sharding import Mesh
from jax.sharding import PartitionSpec as P

BLOCK = 256
SP = ("sp_0", "sp_1")
SP_TP = ("sp_0", "sp_1", "tp")


alpha_scale = 8.0**0.25
rope_base = 10000.0
tiny_stabilizer = 1e-05


def turned_gather(arrays, axis, dims):
    turned = [jnp.moveaxis(a, dim, 0) for a, dim in zip(arrays, dims)]
    both = jnp.concatenate([t.reshape(len(t), -1) for t in turned], axis=1)
    out, at, finished = (lax.all_gather(both, axis, axis=0, tiled=True), 0, [])
    for t, dim in zip(turned, dims):
        piece = out[:, at : at + t[0].size].reshape(-1, *t.shape[1:])
        finished.append(jnp.moveaxis(piece, 0, dim))
        at += t[0].size
    return tuple(finished)


def neutral_like(x, identity):
    return jax.tree.map(
        lambda a, e: jnp.broadcast_to(jnp.asarray(e, a.dtype), a.shape), x, identity
    )


def entering(x, axes, combine, identity):
    before = start = neutral_like(x, identity)
    subtotal = x
    for axis in reversed(axes):
        length, position = (lax.axis_size(axis), lax.axis_index(axis))
        pieces = jax.tree.map(
            lambda part, kind: lax.all_gather(part.astype(kind), axis),
            subtotal,
            (jnp.bfloat16, jnp.bfloat16),
        )
        inside, subtotal = (start, start)
        for k in range(length):
            passed = k < position
            subtotal = combine(
                subtotal, jax.tree.map(lambda part, own: part[k].astype(own.dtype), pieces, x)
            )
            inside = jax.tree.map(lambda new, old: jnp.where(passed, new, old), subtotal, inside)
        before = combine(inside, before)
    return before


def passed_along(x, axis, by):
    length = lax.axis_size(axis)
    pairs = [(i, i + by) for i in range(length) if 0 <= i + by < length]
    return lax.ppermute(x, axis, pairs)


def rotate(vectors, positions):
    head_width = vectors.shape[-1]
    half_width = head_width // 2
    inverse_freq = rope_base ** (-2.0 * jnp.arange(half_width, dtype=jnp.float32) / head_width)
    angles = positions[:, None] * inverse_freq[None, :]
    cosine = jnp.cos(angles)[:, None, :]
    sine_part = jnp.sin(angles)[:, None, :]
    front = vectors[..., :half_width]
    second = vectors[..., half_width:]
    return jnp.concatenate(
        [front * cosine - second * sine_part, front * sine_part + second * cosine], axis=-1
    )


def layer_norm(values, gain, shift):
    average = values.mean(-1, keepdims=True)
    spread = jnp.square(values - average).mean(-1, keepdims=True)
    return (values - average) * lax.rsqrt(spread + tiny_stabilizer) * gain + shift


def block_parts(query_tile, lookup_piece, payload_piece, log_blk):
    cum_log = jnp.cumsum(log_blk, axis=0)
    cum_heads = cum_log.T
    log_gap = cum_heads[:, :, None] - cum_heads[:, None, :]
    offsets = jnp.arange(log_blk.shape[0])
    causal = (offsets[:, None] >= offsets[None, :])[None]
    weight = jnp.where(causal, jnp.exp(jnp.where(causal, log_gap, 0.0)), 0.0)
    score_matrix = jnp.einsum(
        "jka,ska->kjs", query_tile, lookup_piece, preferred_element_type=jnp.float32
    )
    segment_scaling = (score_matrix * weight).astype(jnp.bfloat16)
    within = jnp.einsum(
        "htm,mhe->the", segment_scaling, payload_piece, preferred_element_type=jnp.float32
    )
    block_total = cum_log[-1]
    to_end = jnp.exp(block_total[None, :] - cum_log)
    faded_lookup_vector = (lookup_piece.astype(jnp.float32) * to_end[:, :, None]).astype(
        jnp.bfloat16
    )
    summand_term = jnp.einsum(
        "ajo,ajd->jod", faded_lookup_vector, payload_piece, preferred_element_type=jnp.float32
    )
    scaled_query = (query_tile.astype(jnp.float32) * jnp.exp(cum_log)[:, :, None]).astype(
        jnp.bfloat16
    )
    return (within, scaled_query, summand_term, jnp.exp(block_total))


def causal_conv(rows, edge_rows, taps, shift):
    padded = jnp.concatenate([edge_rows, rows], axis=0).astype(jnp.float32)
    length = rows.shape[0]
    result = shift[None, :] + padded[0:length] * taps[0]
    result = result + padded[1 : length + 1] * taps[1]
    return result + padded[2 : length + 2] * taps[2]


def combine(earlier, later):
    return (earlier[0] * later[0], later[0][:, None, None] * earlier[1] + later[1])


def shards(
    query_proj,
    key_proj,
    value_proj,
    gate_proj,
    log_decay,
    residual,
    out_weight,
    norm_gain,
    norm_bias,
    up_gate,
    up_value,
    conv_weight,
    conv_bias,
    down_weight,
):
    tok_rows = query_proj.shape[0]
    head_count = log_decay.shape[1]
    key_width = query_proj.shape[1] // head_count
    value_width = value_proj.shape[1] // head_count
    full_gate, full_value, full_down = turned_gather(
        (up_gate, up_value, down_weight), SP, (0, 0, 1)
    )
    positions = (lax.axis_index(SP) * tok_rows + jnp.arange(tok_rows)).astype(jnp.float32)
    query_rot = rotate(
        query_proj.astype(jnp.float32).reshape(tok_rows, head_count, key_width), positions
    ).astype(jnp.bfloat16)
    key_rot = (
        rotate(key_proj.astype(jnp.float32).reshape(tok_rows, head_count, key_width), positions)
        * key_width ** (-0.5)
    ).astype(jnp.bfloat16)
    block_count = tok_rows // BLOCK
    asking_segments = query_rot.reshape(block_count, BLOCK, head_count, key_width)
    key_blocks = key_rot.reshape(block_count, BLOCK, head_count, key_width)
    value_blocks = value_proj.reshape(block_count, BLOCK, head_count, value_width)
    log_blocks = log_decay.reshape(block_count, BLOCK, head_count)
    within, scaled_query, summand_term, block_decay = jax.vmap(block_parts)(
        asking_segments, key_blocks, value_blocks, log_blocks
    )

    def absorb(carry_state, pieces):
        return (pieces[1][:, None, None] * carry_state + pieces[0], None)

    zero_state = jnp.zeros((head_count, key_width, value_width), jnp.float32)
    own_state, _ = lax.scan(absorb, zero_state, (summand_term, block_decay))
    own_decay = jnp.prod(block_decay, axis=0)
    _, incoming = entering(
        (own_decay, own_state), SP, combine, (jnp.ones_like(own_decay), zero_state)
    )

    def advance(carry_state, pieces):
        carried = jnp.einsum(
            "thd,hde->the",
            pieces[0],
            carry_state.astype(jnp.bfloat16),
            preferred_element_type=jnp.float32,
        )
        return (pieces[2][:, None, None] * carry_state + pieces[1], carried)

    _, carried = lax.scan(advance, incoming, (scaled_query, summand_term, block_decay))
    mixed_heads = (within + carried).reshape(tok_rows, head_count, value_width)
    average = mixed_heads.mean(-1, keepdims=True)
    spread = jnp.square(mixed_heads - average).mean(-1, keepdims=True)
    standardized_rows = (mixed_heads - average) * lax.rsqrt(spread + tiny_stabilizer)
    gate_heads = gate_proj.astype(jnp.float32).reshape(tok_rows, head_count, value_width)
    gated_rows = (
        (jax.nn.silu(gate_heads) * standardized_rows)
        .astype(jnp.bfloat16)
        .reshape(tok_rows, head_count * value_width)
    )
    own_count = tok_rows // lax.axis_size("tp")
    partial_rows = jnp.dot(gated_rows, out_weight, preferred_element_type=jnp.float32)
    attended = lax.psum(partial_rows.astype(jnp.bfloat16), "tp").astype(jnp.float32)
    whole_rows = layer_norm(
        alpha_scale * residual.astype(jnp.float32) + attended, norm_gain[0], norm_bias[0]
    ).astype(jnp.bfloat16)
    normed_own = lax.dynamic_slice_in_dim(
        whole_rows, lax.axis_index("tp") * own_count, own_count, 0
    )
    gate_up = jnp.dot(whole_rows, full_gate, preferred_element_type=jnp.float32)
    value_up = jnp.dot(whole_rows, full_value, preferred_element_type=jnp.float32)
    gate_up = gate_up.astype(jnp.bfloat16)
    value_up = value_up.astype(jnp.bfloat16)
    gate_edge, value_edge = passed_along((gate_up[tok_rows - 2 :], value_up[tok_rows - 2 :]), SP, 1)
    gate_conv = causal_conv(gate_up, gate_edge, conv_weight[0], conv_bias[0])
    value_conv = causal_conv(value_up, value_edge, conv_weight[1], conv_bias[1])
    activated = (jax.nn.gelu(gate_conv) * value_conv).astype(jnp.bfloat16)
    partial_ffn = jnp.dot(activated, full_down, preferred_element_type=jnp.float32)
    ffn_out = lax.psum_scatter(
        partial_ffn.astype(jnp.bfloat16), "tp", scatter_dimension=0, tiled=True
    ).astype(jnp.float32)
    return layer_norm(
        alpha_scale * normed_own.astype(jnp.float32) + ffn_out, norm_gain[1], norm_bias[1]
    ).astype(jnp.bfloat16)


def solution(mesh):
    torus = Mesh(mesh.devices.reshape(4, 4, mesh.shape["tp"]), ("sp_0", "sp_1", "tp"))
    return jax.shard_map(
        shards,
        mesh=torus,
        in_specs=(
            P(SP, "tp"),
            P(SP, "tp"),
            P(SP, "tp"),
            P(SP, "tp"),
            P(SP, "tp"),
            P(SP, None),
            P("tp", None),
            P(),
            P(),
            P(SP, "tp"),
            P(SP, "tp"),
            P(None, None, "tp"),
            P(None, "tp"),
            P("tp", SP),
        ),
        out_specs=P(SP_TP, None),
        check_vma=False,
    )
```

profile of v0, /device:TPU:1, one launch (start us, length us, event | category | flops | bytes accessed | tf_op | source)
XLA Modules:
  0.0 285.5 jit_solution(7384815758810816143)
XLA Ops:
  7.4 2.4 reduce-window.6
  11.8 3.1 %fusion.56 = (bf16[1024,1,128]{2,0,1:T(8,128)(2,1)S(1)}, bf16[1024,1,128]{2,0,1:T(8,128)(2,1)}, f32[1024,1,128]{2,0,1:T(8,128)S(1)}, f32[1024,1,128]{2,0,1:T(8,128)S(1)}) fusion(f32[1024,1,256]{2,0,1:T(8,128)S(1)} %get-tuple-element.170, f32[128]{0:T(128)S(1)} %multiply_power_fusion, f32[1024]{0:T(1024)S(1)} %add_convert_fusion.2, ...), kind=kLoop, calls=%fused_computation.87 | loop fusion | flops 1966080 | bytes 3674624 | tf_op jit(solution)/shard_map/convert.17
  15.7 2.0 convolution_bitcast_fusion.1
  17.7 9.8 %while.24 = (s32[]{:T(128)}, f32[1,256,512]{2,1,0:T(8,128)S(1)}, f32[4,1]{0,1:T(1,128)S(1)}, f32[4,1,256,512]{3,2,1,0:T(8,128)}, s32[]{:T(128)}, /*index=5*/s32[]{:T(128)}) while((s32[]{:T(128)}, f32[1,256,512]{2,1,0:T(8,128)S(1)}, f32[4,1]{0,1:T(1,128)S(1)}, f32[4,1,256,512]{3,2,1,0:T(8,128)}, s32[]{:T(128)}, ...), condition=%wide.region_4.5_spmd.clone, body=%wide.region_3.4_spmd.clone.sunk | while | flops 393219 | bytes 1572971 | solution.py:165
  31.0 9.5 %all-reduce = bf16[4]{0:T(256)(128)(2,1)S(1)} all-reduce(bf16[4]{0:T(256)(128)(2,1)S(1)} %dynamic-update-slice), channel_id=1, replica_groups=mesh['sp_0'=4,'sp_1'=4,'tp'=8] {'sp_1'}, use_global_device_ids=true, to_apply=%add | all-reduce | flops 4 | bytes 16
  41.8 11.8 %all-gather.10.cloned.1.call-done = bf16[4,256,512]{2,1,0:T(8,128)(2,1)} async-done(((bf16[1,256,512]{2,1,0:T(8,128)(2,1)}), bf16[4,256,512]{2,1,0:T(8,128)(2,1)}) %all-gather.10.cloned.1.call-update) | async-done | bytes 1048592 | tf_op jit(solution)/shard_map/all_gather | solution.py:40
  53.7 4.0 %fusion.70 = bf16[1,1,256,512]{3,2,1,0:T(8,128)(2,1)} fusion(f32[]{:T(128)} %bitcast.39, f32[]{:T(128)} %bitcast.40, f32[]{:T(128)} %bitcast.41, f32[]{:T(128)} %bitcast.42, bf16[4,256,512]{2,1,0:T(8,128)(2,1)} %all-gather.10.cloned.1.call-done), kind=kLoop, calls=%fused_computation.102 | loop fusion | flops 1572864 | bytes 1310736 | tf_op jit(solution)/shard_map/convert_element_type | solution.py:40
  60.5 8.9 %all-reduce.1 = bf16[4]{0:T(256)(128)(2,1)S(1)} all-reduce(bf16[4]{0:T(256)(128)(2,1)S(1)} %dynamic-update-slice.1), channel_id=2, replica_groups=mesh['sp_0'=4,'sp_1'=4,'tp'=8] {'sp_0'}, use_global_device_ids=true, to_apply=%add.1 | all-reduce | flops 4 | bytes 16
  75.2 1.9 fusion.61
  77.1 5.3 %all-gather.6.cloned.1.call-done = bf16[4,1,256,512]{3,2,1,0:T(8,128)(2,1)} async-done(((bf16[1,1,256,512]{3,2,1,0:T(8,128)(2,1)}), bf16[4,1,256,512]{3,2,1,0:T(8,128)(2,1)}) %all-gather.6.cloned.1.call-update) | async-done | bytes 1048592 | tf_op jit(solution)/shard_map/all_gather | solution.py:40
  82.4 3.9 %fusion.69 = f32[1,256,512]{2,1,0:T(8,128)S(1)} fusion(bf16[4,1,256,512]{3,2,1,0:T(8,128)(2,1)} %all-gather.6.cloned.1.call-done, f32[]{:T(128)} %bitcast.39, f32[]{:T(128)} %bitcast.40, f32[]{:T(128)} %bitcast.41, f32[]{:T(128)} %bitcast.42, f32[]{:T(128)} %bitcast.33, f32[]{:T(128)S(6)} %convert.26, f32[]{:T(128)S(6)} %convert.27, f32[]{:T(128)} %bitcast.38, ...), kind=kLoop, calls=%fused_computation.99 | loop fusion | flops 4194304 | bytes 2621484 | tf_op jit(solution)/shard_map/add | solution.py:118
  86.4 17.8 %while.23 = (s32[]{:T(128)}, f32[1,256,512]{2,1,0:T(8,128)S(1)}, f32[4,256,1,512]{3,1,2,0:T(8,128)}, f32[4,1]{0,1:T(1,128)S(1)}, f32[4,1,256,512]{3,2,1,0:T(8,128)}, /*index=5*/bf16[4,256,1,256]{3,1,2,0:T(8,128)(2,1)}, s32[]{:T(128)}) while((s32[]{:T(128)}, f32[1,256,512]{2,1,0:T(8,128)S(1)}, f32[4,256,1,512]{3,1,2,0:T(8,128)}, ...), condition=%wide.region_6.7_spmd, body=%wide.region_5.6_spmd.sunk | while | flops 67502080 | bytes 2753641 | solution.py:180
  87.0 1.9 fusion.117
  88.9 1.9 bitcast_add_fusion.7
  91.4 1.9 fusion.117
  95.9 1.9 fusion.117
  100.3 1.9 fusion.117
  104.1 4.2 %fusion.101 = (f32[4,256]{1,0:T(4,128)S(1)}, f32[4,256,1,512]{3,1,0,2:T(8,128)}) fusion(f32[4,256,1,512]{3,1,2,0:T(8,128)} %get-tuple-element.60, bf16[4,256,512]{2,1,0:T(8,128)(2,1)} %bitcast.150, bf16[4,256,128]{2,1,0:T(8,128)(2,1)} %bitcast.155, bf16[4,256,128]{2,1,0:T(8,128)(2,1)S(1)} %bitcast.153, f32[4,256]{1,0:T(4,128)S(1)} %get-tuple-element.135, ...), kind=kOutput, calls=%fused_computation.158 | convolution fusion | flops 406846464 | bytes 6889472 | tf_op jit(solution)/shard_map/vmap(htm,mhe->the)/dot_general | solution.py:92
  108.4 2.1 multiply_reduce_fusion.1
  110.6 2.2 fusion.32
  112.8 4.3 %convolution_convert_fusion.1 = bf16[1024,2048]{1,0:T(8,128)(2,1)} fusion(bf16[1024,512]{1,0:T(8,128)(2,1)S(1)} %fusion.32, bf16[512,2048]{1,0:T(8,128)(2,1)S(1)} %copy-done), kind=kOutput, calls=%fused_computation.18 | convolution fusion | flops 2149580800 | bytes 7340032 | tf_op jit(solution)/shard_map/dot_general | solution.py:192
  119.4 71.7 %all-reduce.4.cloned.1.call-done = bf16[1024,2048]{1,0:T(8,128)(2,1)} async-done(((bf16[1024,2048]{1,0:T(8,128)(2,1)}), bf16[1024,2048]{1,0:T(8,128)(2,1)}) %all-reduce.4.cloned.1.call-update) | async-done | bytes 4194320 | tf_op jit(solution)/shard_map/psum | solution.py:193
  191.1 5.1 %fusion.6 = f32[1024]{0:T(1024)S(1)} fusion(bf16[1024,2048]{1,0:T(8,128)(2,1)} %all-reduce.4.cloned.1.call-done, bf16[1024,2048]{1,0:T(8,128)(2,1)} %param.23), kind=kLoop, calls=%fused_computation.15 | loop fusion | flops 10484736 | bytes 8392704 | tf_op jit(solution)/shard_map/reduce_sum | solution.py:76
  197.2 2.4 multiply_reduce_fusion
  199.6 4.0 %add_convert_fusion = bf16[1024,2048]{1,0:T(8,128)(2,1)} fusion(bf16[1024,2048]{1,0:T(8,128)(2,1)S(1)} %copy-done.2, bf16[1024,2048]{1,0:T(8,128)(2,1)S(1)} %copy-done.1, f32[2048]{0:T(1024)S(1)} %bitcast.164, f32[2048]{0:T(1024)S(1)} %bitcast.163, f32[1024]{0:T(1024)S(1)} %add_rsqrt_fusion, f32[1024]{0:T(1024)S(1)} %broadcast_multiply_fusion), kind=kLoop, calls=%fused_computation.12 | loop fusion | flops 18874368 | bytes 12607488 | tf_op jit(solution)/shard_map/convert_element_type | solution.py:196
  203.6 6.4 %fusion.33 = bf16[1024,704]{0,1:T(8,128)(2,1)S(1)} fusion(bf16[1024,2048]{1,0:T(8,128)(2,1)} %add_convert_fusion, bf16[2048,2112]{0,1:T(8,128)(2,1)} %all-gather.8.cloned.1.call-done), kind=kOutput, calls=%fused_computation.56 | convolution fusion | flops 2953510912 | bytes 8519680 | tf_op jit(solution)/shard_map/dot_general | solution.py:200
  210.1 3.0 %collective-permute-start = (bf16[2,704]{0,1:T(8,128)(2,1)S(1)}, bf16[2,704]{0,1:T(8,128)(2,1)S(1)}, u32[]{:S(2)}, u32[]{:S(2)}) collective-permute-start(bf16[2,704]{0,1:T(8,128)(2,1)S(1)} %slice.226), channel_id=1, source_target_pairs={{0,8},{8,16},{16,24},{24,32},{32,40},{40,48},{48,56},{56,64},{64,7... | collective-permute-start | bytes 8456 | tf_op jit(solution)/shard_map/ppermute | solution.py:58
  213.2 5.0 %fusion.36 = bf16[1024,704]{0,1:T(8,128)(2,1)S(1)} fusion(bf16[1024,2048]{1,0:T(8,128)(2,1)S(1)} %copy-done.4, bf16[2048,2112]{0,1:T(8,128)(2,1)} %all-gather.8.cloned.1.call-done), kind=kOutput, calls=%fused_computation.57 | convolution fusion | flops 2953510912 | bytes 8519680 | tf_op jit(solution)/shard_map/dot_general | solution.py:201
  218.3 3.3 %collective-permute-start.1 = (bf16[2,704]{0,1:T(8,128)(2,1)S(1)}, bf16[2,704]{0,1:T(8,128)(2,1)S(1)}, u32[]{:S(2)}, u32[]{:S(2)}) collective-permute-start(bf16[2,704]{0,1:T(8,128)(2,1)S(1)} %slice.231), channel_id=1, source_target_pairs={{0,8},{8,16},{16,24},{24,32},{32,40},{40,48},{48,56},{56,64},{64,7... | collective-permute-start | bytes 8456 | tf_op jit(solution)/shard_map/ppermute | solution.py:58
  224.6 10.0 %convolution_convert_fusion = bf16[1024,2048]{1,0:T(8,128)(2,1)} fusion(bf16[2048,2112]{0,1:T(8,128)(2,1)} %all-gather.8.cloned.1.call-done, f32[1026,704]{0,1:T(8,128)S(1)} %maximum_convert_fusion.1, f32[1026,704]{0,1:T(8,128)S(1)} %maximum_convert_fusion, f32[704]{0:T(1024)S(1)} %get-tuple-element.110, f32[704]{0:T(1024)S(1)} %get-tuple-element.111, ...), kind=kOutput, calls=%fused_computation.17 | convolution fusion | flops 2970746880 | bytes 24412160 | tf_op jit(solution)/shard_map/dot_general | solution.py:208
  234.6 38.4 %reduce-scatter.2.cloned.1.call-done = bf16[128,2048]{1,0:T(8,128)(2,1)} async-done(((bf16[1024,2048]{1,0:T(8,128)(2,1)}), bf16[128,2048]{1,0:T(8,128)(2,1)}) %reduce-scatter.2.cloned.1.call-update) | async-done | bytes 524304 | tf_op jit(solution)/shard_map/reduce_scatter | solution.py:209
  276.0 2.3 add_convert_fusion.1
  (106 shorter events, 37.7 us)
Async XLA Ops:
  7.4 105.4 %copy-start = (bf16[512,2048]{1,0:T(8,128)(2,1)S(1)}, bf16[512,2048]{1,0:T(8,128)(2,1)}, u32[]{:S(2)}) copy-start(bf16[512,2048]{1,0:T(8,128)(2,1)} %param.24) | copy-start | bytes 6291460
  7.4 46.3 %all-gather.10.cloned.1.call-start = ((), (), s32[]{:S(2)}) async-start(), calls=%async_computation.5 | async-start | bytes 1310720 | tf_op jit(solution)/shard_map/all_gather | solution.py:40
  10.4 5.3 %copy-start.6 = (bf16[1024,512]{1,0:T(8,128)(2,1)S(1)}, bf16[1024,512]{1,0:T(8,128)(2,1)}, u32[]{:S(2)}) copy-start(bf16[1024,512]{1,0:T(8,128)(2,1)} %param.20) | copy-start | bytes 3145732
  14.9 0.8 copy-start.5
  17.7 10.6 %copy-start.15 = (u32[128]{0:T(128)S(1)}, u32[128]{0:T(128)}, u32[]{:S(2)}) copy-start(u32[128]{0:T(128)} %constant.102) | copy-start | bytes 1540
  17.7 40.0 %copy-start.14 = (u32[128]{0:T(128)S(1)}, u32[128]{0:T(128)}, u32[]{:S(2)}) copy-start(u32[128]{0:T(128)} %constant.107) | copy-start | bytes 1540
  28.3 54.2 %all-gather.6.cloned.1.call-start = ((), (), s32[]{:S(2)}) async-start(), calls=%async_computation.1 | async-start | bytes 1310720 | tf_op jit(solution)/shard_map/all_gather | solution.py:40
  57.6 133.5 %all-reduce.4.cloned.1.call-start = ((), (), s32[]{:S(2)}) async-start(), calls=%async_computation.2 | async-start | bytes 8388608 | tf_op jit(solution)/shard_map/psum | solution.py:193
  108.4 2.2 copy-start.3
  117.1 0.9 copy-start.7
  117.1 1.0 copy-start.8
  117.1 1.1 copy-start.9
  117.1 2.2 copy-start.13
  117.1 2.2 copy-start.10
  117.1 2.3 copy-start.11
  117.1 2.3 copy-start.12
  117.1 86.5 %all-gather.8.cloned.1.call-start = ((), (), s32[]{:S(2)}) async-start(), calls=%async_computation.3 | async-start | bytes 9191424 | tf_op jit(solution)/shard_map/all_gather | solution.py:20
  119.0 154.0 %reduce-scatter.2.cloned.1.call-start = ((), (), s32[]{:S(2)}) async-start(), calls=%async_computation.4 | async-start | bytes 4718592 | tf_op jit(solution)/shard_map/reduce_scatter | solution.py:209
  191.1 5.1 %copy-start.1 = (bf16[1024,2048]{1,0:T(8,128)(2,1)S(1)}, bf16[1024,2048]{1,0:T(8,128)(2,1)}, u32[]{:S(2)}) copy-start(bf16[1024,2048]{1,0:T(8,128)(2,1)} %param.23) | copy-start | bytes 12582916
  191.1 6.0 %copy-start.2 = (bf16[1024,2048]{1,0:T(8,128)(2,1)S(1)}, bf16[1024,2048]{1,0:T(8,128)(2,1)}, u32[]{:S(2)}) copy-start(bf16[1024,2048]{1,0:T(8,128)(2,1)} %all-reduce.4.cloned.1.call-done) | copy-start | bytes 12582916
  203.6 9.6 %copy-start.4 = (bf16[1024,2048]{1,0:T(8,128)(2,1)S(1)}, bf16[1024,2048]{1,0:T(8,128)(2,1)}, u32[]{:S(2)}) copy-start(bf16[1024,2048]{1,0:T(8,128)(2,1)} %add_convert_fusion) | copy-start | bytes 12582916
  210.1 11.5 %collective-permute-start = (bf16[2,704]{0,1:T(8,128)(2,1)S(1)}, bf16[2,704]{0,1:T(8,128)(2,1)S(1)}, u32[]{:S(2)}, u32[]{:S(2)}) collective-permute-start(bf16[2,704]{0,1:T(8,128)(2,1)S(1)} %slice.226), channel_id=1, source_target_pairs={{0,8},{8,16},{16,24},{24,32},{32,40},{40,48},{48,56},{56,64},{64,7... | collective-permute-start | bytes 8456 | tf_op jit(solution)/shard_map/ppermute | solution.py:58
  218.3 5.5 %collective-permute-start.1 = (bf16[2,704]{0,1:T(8,128)(2,1)S(1)}, bf16[2,704]{0,1:T(8,128)(2,1)S(1)}, u32[]{:S(2)}, u32[]{:S(2)}) collective-permute-start(bf16[2,704]{0,1:T(8,128)(2,1)S(1)} %slice.231), channel_id=1, source_target_pairs={{0,8},{8,16},{16,24},{24,32},{32,40},{40,48},{48,56},{56,64},{64,7... | collective-permute-start | bytes 8456 | tf_op jit(solution)/shard_map/ppermute | solution.py:58
Sparse Core Ops, SparseCore 0:
  28.4 25.2 all-gather.9
  57.8 24.6 all-gather.5
  117.3 73.8 all-reduce.3
  234.7 38.2 reduce-scatter.1
Sparse Core Ops, SparseCore 1:
  119.7 79.2 all-gather.7
where the time goes:
time: 289 us; the launch traced here: 285 us
  waiting for transfers between devices  129 us (45%)
  other arithmetic  58.1 us (20%)
  matrix products  39.6 us (14%)
  between operations  20.6 us (7%)
  blocking collectives  18.5 us (6%)
  local copies, waits for them, and re-layouts  13.1 us (5%)
  starting transfers between devices  6.72 us (2%)
    psum x1, waiting for transfers between devices, shards(): lax.psum(partial_rows.astype(jnp.bfloat16), 'tp').astype(jnp.float32)  71.7 us
    reduce_scatter x1, waiting for transfers between devices, shards(): lax.psum_scatter(partial_ffn.astype(jnp.bfloat16), 'tp', scatter_dimensio...  38.4 us
    unnamed x2, blocking collectives  18.5 us
    all_gather x2, waiting for transfers between devices, entering(): lax.all_gather(part.astype(kind), axis)  17.1 us
    dot_general x1, matrix products, shards(): jnp.dot(activated, full_down, preferred_element_type=jnp.float32)  9.97 us
    dot_general x4, matrix products, advance(): jnp.einsum('thd,hde->the', pieces[0], carry_state.astype(jnp.bfloat16), p...  7.74 us
    add x4, other arithmetic, advance(): return (pieces[2][:, None, None] * carry_state + pieces[1], carried)  7.52 us
    add x4, other arithmetic, absorb(): return (pieces[1][:, None, None] * carry_state + pieces[0], None)  7.35 us
  transfers between devices with their start and end apart: 7, of which 5 were waited for; matrix products, arithmetic and copies ran while one was open for 10% of the time, Pallas kernels for 0%

commit v1 on v0

v1 whole, which is shorter than its diff:
```python
import functools

import jax
import jax.numpy as jnp
import numpy as np
from jax import lax
from jax.experimental import pallas as pl
from jax.experimental.pallas import tpu as pltpu
from jax.sharding import Mesh
from jax.sharding import PartitionSpec as P

F32 = jnp.float32
BF16 = jnp.bfloat16
HIGH = lax.Precision.HIGHEST
MESH = pl.DeviceIdType.MESH
ALPHA = 8.0**0.25
EPS = 1e-05
NSP = 16
BLK = 256
FF = 704
FFP = 768
NT = (((1,), (1,)), ((), ()))
TN = (((0,), (0,)), ((), ()))


def position_tables():
    freq = 10000.0 ** (-2.0 * np.arange(128, dtype=np.float64) / 256.0)
    inner = np.arange(BLK, dtype=np.float64)[:, None] * freq[None]
    start = np.arange(4 * NSP, dtype=np.float64)[:, None] * BLK * freq[None]
    ti = np.stack([np.cos(inner), np.sin(inner)]).astype(np.float32)
    tb = np.concatenate(
        [np.cos(start).reshape(NSP, 4, 128), np.sin(start).reshape(NSP, 4, 128)], axis=1
    ).astype(np.float32)
    return ti, tb


def body(
    q_h, k_h, v_h, g_h, log_ref, res_h, ow_h, gain_ref, bias_ref, ug_h, uv_h, taps_ref, dw_h,
    ti_ref, tb_ref, o_ref,
    qv, kv, vv, gv, rv, owv, ust, wu, wd,
    lsc, crow, ccol, dpre, kr, sq, loc, within, gr,
    ssend, srecv, rsend, inc,
    part, d2, cb, ra, rb, rl, rr,
    xb, ub, act, halo,
    in_sem, ss_s, ss_r, rs_s, rs_r, wg_s, wg_r, d2_s, d2_r, x_s, x_r, ag_s, ag_r, h_s, h_r,
):
    z, y, x, c = (lax.axis_index(a) for a in ("z", "y", "x", "c"))
    me = z * 4 + y
    t = x * 2 + c
    xr, xl, xo = lax.rem(x + 1, 4), lax.rem(x + 3, 4), lax.rem(x + 2, 4)

    def at(axis, value):
        return {axis: value}

    SIB = at("c", 1 - c)
    XR, XL = at("x", xr), at("x", xl)

    def remote(src, dst, ssem, rsem, dev):
        return pltpu.make_async_remote_copy(
            src_ref=src, dst_ref=dst, send_sem=ssem, recv_sem=rsem, device_id=dev,
            device_id_type=MESH,
        )

    loads = [
        (ug_h.at[0:640], ust.at[0:640]),
        (uv_h.at[0:640], ust.at[640:1280]),
        (ug_h.at[640:704], ust.at[1280:1344]),
        (uv_h.at[640:704], ust.at[1344:1408]),
        (dw_h, wd.at[0:FF, pl.ds(pl.multiple_of(me * 128, 128), 128)]),
        (k_h, kv),
        (v_h, vv),
        (q_h, qv),
        (g_h, gv),
        (ow_h, owv),
        (res_h.at[pl.ds(pl.multiple_of(t * 128, 128), 128)], rv),
    ]
    loads = [pltpu.make_async_copy(s, d, in_sem.at[i]) for i, (s, d) in enumerate(loads)]
    for load in loads:
        load.start()

    barrier = pltpu.get_barrier_semaphore()

    def sp_peer(i):
        j = lax.rem(me + i, NSP)
        return j, {"z": lax.div(j, 4), "y": lax.rem(j, 4)}

    def greet(i, carry):
        _, dev = sp_peer(i)
        pl.semaphore_signal(barrier, inc=1, device_id=dev, device_id_type=MESH)
        return carry

    lax.fori_loop(1, NSP, greet, 0)
    for dev in (SIB, XR, XL):
        pl.semaphore_signal(barrier, inc=1, device_id=dev, device_id_type=MESH)

    yr, yl, yo = lax.rem(y + 1, 4), lax.rem(y + 3, 4), lax.rem(y + 2, 4)
    zr, zl, zo = lax.rem(z + 1, 4), lax.rem(z + 3, 4), lax.rem(z + 2, 4)
    YR, YL, ZR, ZL = at("y", yr), at("y", yl), at("z", zr), at("z", zl)

    def up_piece(zz, yy, lo, n):
        return wu.at[zz * 4 + yy, lo * 16 : (lo + n) * 16, :]

    def dn_piece(zz, yy, lo, n):
        col = pl.multiple_of((zz * 4 + yy) * 128, 128)
        return wd.at[lo * 88 : (lo + n) * 88, pl.ds(col, 128)]

    def gather(g, piece):
        def put(n, zz, yy, lo, cnt, dev):
            p = piece(zz, yy, lo, cnt)
            remote(p, p, wg_s.at[g, n], wg_r.at[g, n], dev).start()

        def got(n, zz, yy, lo, cnt):
            p = piece(zz, yy, lo, cnt)
            remote(p, p, wg_s.at[g, n], wg_r.at[g, n], YR).wait_recv()

        def s0():
            put(0, z, y, 0, 4, YR)
            put(1, z, y, 0, 4, YL)
            put(2, z, y, 4, 4, ZR)
            put(3, z, y, 4, 4, ZL)

        def s0b():
            put(4, z, y, 0, 4, ZR)
            put(5, z, y, 0, 4, ZL)
            put(6, z, y, 4, 4, YR)
            put(7, z, y, 4, 4, YL)

        def s1():
            got(0, z, yl, 0, 4)
            put(8, z, yl, 0, 2, YR)
            got(1, z, yr, 0, 4)
            put(9, z, yr, 2, 2, YL)
            got(2, zl, y, 4, 4)
            put(10, zl, y, 4, 2, ZR)
            got(3, zr, y, 4, 4)
            put(11, zr, y, 6, 2, ZL)
            put(12, z, yl, 0, 4, ZR)
            put(13, z, yl, 0, 4, ZL)
            put(14, zl, y, 4, 4, YR)
            put(15, zl, y, 4, 4, YL)
            put(16, z, yr, 0, 4, ZR)
            put(17, z, yr, 0, 4, ZL)
            put(18, zr, y, 4, 4, YR)
            put(19, zr, y, 4, 4, YL)

        def s2():
            got(8, z, yo, 0, 2)
            got(9, z, yo, 2, 2)
            got(10, zo, y, 4, 2)
            got(11, zo, y, 6, 2)
            put(20, z, yo, 0, 4, ZR)
            put(21, z, yo, 0, 4, ZL)
            put(22, zo, y, 4, 4, YR)
            put(23, zo, y, 4, 4, YL)

        def s3(m):
            n = (4, 12, 16, 20)[m]
            w = 24 + 4 * m
            ym, zm = (y, yl, yr, yo)[m], (z, zl, zr, zo)[m]
            nb = n + 2
            got(n, zl, ym, 0, 4)
            put(w, zl, ym, 0, 2, ZR)
            got(n + 1, zr, ym, 0, 4)
            put(w + 1, zr, ym, 2, 2, ZL)
            got(nb, zm, yl, 4, 4)
            put(w + 2, zm, yl, 4, 2, YR)
            got(nb + 1, zm, yr, 4, 4)
            put(w + 3, zm, yr, 6, 2, YL)

        def s4():
            for m in range(4):
                w = 24 + 4 * m
                ym, zm = (y, yl, yr, yo)[m], (z, zl, zr, zo)[m]
                got(w, zo, ym, 0, 2)
                got(w + 1, zo, ym, 2, 2)
                got(w + 2, zm, yo, 4, 2)
                got(w + 3, zm, yo, 6, 2)

        def drain():
            for n in range(40):
                cnt = 2 if 8 <= n < 12 or n >= 24 else 4
                p = piece(z, y, 0, cnt)
                remote(p, p, wg_s.at[g, n], wg_r.at[g, n], YR).wait_send()

        return s0, s0b, s1, s2, s3, s4, drain

    u0, u0b, u1, u2, u3, u4, udrain = gather(0, up_piece)
    n0, n0b, n1, n2, n3, n4, ndrain = gather(1, dn_piece)

    lsc[...] = jnp.zeros((8, 256), F32)
    for b in range(4):
        lsc[b : b + 1, 0:128] = log_ref[2 * b : 2 * b + 1, :]
        lsc[b : b + 1, 128:256] = log_ref[2 * b + 1 : 2 * b + 2, :]
    ri = lax.broadcasted_iota(jnp.int32, (BLK, BLK), 0)
    ci = lax.broadcasted_iota(jnp.int32, (BLK, BLK), 1)
    causal = ri >= ci
    tri = jnp.where(causal, 1.0, 0.0).astype(F32)
    logs = lsc[...]
    crow[...] = lax.dot_general(logs, tri, NT, precision=HIGH, preferred_element_type=F32)
    ccol[...] = lax.dot_general(tri, logs, NT, precision=HIGH, preferred_element_type=F32)

    wd[FF:FFP, :] = jnp.zeros((FFP - FF, 2048), BF16)

    for i in range(4):
        loads[i].wait()
    for n in range(11):
        tile = ust[n * 128 : (n + 1) * 128, :].astype(F32)
        wu[me, :, n * 128 : (n + 1) * 128] = tile.T.astype(BF16)
    pl.semaphore_wait(barrier, NSP + 2)
    u0()
    u0b()

    base = tb_ref[me]

    def turned(ref, b):
        ci_, si_ = ti_ref[0], ti_ref[1]
        cb_, sb_ = base[b : b + 1, :], base[4 + b : 5 + b, :]
        cos = cb_ * ci_ - sb_ * si_
        sin = sb_ * ci_ + cb_ * si_
        front = ref[b * BLK : (b + 1) * BLK, 0:128].astype(F32)
        second = ref[b * BLK : (b + 1) * BLK, 128:256].astype(F32)
        return front * cos - second * sin, front * sin + second * cos

    loads[5].wait()
    loads[6].wait()
    decay = jnp.ones((1, 1), F32)
    for b in range(4):
        front, second = turned(kv, b)
        front = (front * 0.0625).astype(BF16)
        second = (second * 0.0625).astype(BF16)
        kr[b, :, 0:128] = front
        kr[b, :, 128:256] = second
        total = crow[b : b + 1, 255:256]
        to_end = jnp.exp(total - ccol[:, b : b + 1])
        faded = jnp.concatenate([front, second], axis=1).astype(F32) * to_end
        state = lax.dot_general(
            faded.astype(BF16), vv[b * BLK : (b + 1) * BLK, :], TN, preferred_element_type=F32
        )
        step = jnp.exp(total)
        dpre[b] = jnp.broadcast_to(decay, (8, 128))
        decay = decay * step
        if b == 0:
            loc[b] = jnp.zeros((BLK, 512), F32)
            loc[b + 1] = state
        else:
            loc[b + 1] = step * loc[b] + state

    hi = decay.astype(BF16)
    mid = (decay - hi.astype(F32)).astype(BF16)
    low = (decay - hi.astype(F32) - mid.astype(F32)).astype(BF16)
    row = lax.broadcasted_iota(jnp.int32, (16, 128), 0)
    tag = jnp.where(
        row == 0,
        hi.astype(F32),
        jnp.where(row == 1, mid.astype(F32), jnp.where(row == 2, low.astype(F32), 0.0)),
    ).astype(BF16)
    for j in range(NSP):
        ssend[j, :, 0:512] = loc[4, j * 16 : (j + 1) * 16, :].astype(BF16)
        ssend[j, :, 512:640] = tag
    srecv[me] = ssend[me]

    def scatter(i, carry):
        j, dev = sp_peer(i)
        remote(ssend.at[j], srecv.at[me], ss_s.at[j], ss_r.at[me], dev).start()
        return carry

    lax.fori_loop(1, NSP, scatter, 0)
    u1()

    loads[7].wait()
    for b in range(4):
        front, second = turned(qv, b)
        qr = jnp.concatenate([front, second], axis=1).astype(BF16)
        column = ccol[:, b : b + 1]
        sq[b] = (qr.astype(F32) * jnp.exp(column)).astype(BF16)
        scores = lax.dot_general(qr, kr[b], NT, preferred_element_type=F32)
        gap = column - crow[b : b + 1, :]
        weight = jnp.where(causal, jnp.exp(jnp.where(causal, gap, 0.0)), 0.0)
        within[b] = jnp.dot(
            (scores * weight).astype(BF16),
            vv[b * BLK : (b + 1) * BLK, :],
            preferred_element_type=F32,
        )

    def scattered(i, carry):
        j, dev = sp_peer(i)
        remote(ssend.at[j], srecv.at[j], ss_s.at[j], ss_r.at[j], dev).wait_recv()
        return carry

    lax.fori_loop(1, NSP, scattered, 0)
    acc = jnp.zeros((16, 512), F32)
    for d in range(NSP):
        rsend[d] = acc.astype(BF16)
        if d < NSP - 1:
            tags = srecv[d, :, 512:640].astype(F32)
            factor = tags[0:1, 0:1] + tags[1:2, 0:1] + tags[2:3, 0:1]
            acc = factor * acc + srecv[d, :, 0:512].astype(F32)
    inc[me] = rsend[me]

    def give_back(i, carry):
        j, dev = sp_peer(i)
        remote(rsend.at[j], inc.at[me], rs_s.at[j], rs_r.at[me], dev).start()
        return carry

    lax.fori_loop(1, NSP, give_back, 0)
    u2()
    u3(0)

    def given(i, carry):
        j, dev = sp_peer(i)
        remote(rsend.at[j], inc.at[j], rs_s.at[j], rs_r.at[j], dev).wait_recv()
        return carry

    lax.fori_loop(1, NSP, given, 0)

    order = (xo, xr, xl, x)

    def reduce_scatter(s, compute, polls):
        def pair(j):
            return remote(
                part.at[s, j, 1 - c], d2.at[s, j], d2_s.at[s, j], d2_r.at[s, j], SIB
            )

        def merged(j, lo, hi, extra=None):
            def rows(i, carry):
                r = pl.ds(pl.multiple_of(i * 32, 32), 32)
                v = part[s, j, c, r, lo:hi].astype(F32) + d2[s, j, r, lo:hi].astype(F32)
                if extra is not None:
                    v = v + extra[s, r, :].astype(F32)
                cb[s, j, r, lo:hi] = v.astype(BF16)
                return carry

            lax.fori_loop(0, 4, rows, 0)

        def across(n, src, dst, dev):
            return remote(src, dst, x_s.at[s, n], x_r.at[s, n], dev)

        L, R = slice(0, 1024), slice(1024, 2048)
        a_out = across(0, cb.at[s, 0, :, L], ra.at[s], XR)
        b_out = across(1, cb.at[s, 0, :, R], rb.at[s], XL)
        r_late = across(2, cb.at[s, 1, :, L], rl.at[s, :, L], XR)
        r_soon = across(3, cb.at[s, 1, :, R], rl.at[s, :, R], XR)
        l_soon = across(4, cb.at[s, 2, :, L], rr.at[s, :, L], XL)
        l_late = across(5, cb.at[s, 2, :, R], rr.at[s, :, R], XL)

        compute(0, order[0])
        pair(0).start()
        polls[0]()
        compute(1, order[1])
        pair(1).start()
        pair(0).wait_recv()
        merged(0, 0, 1024)
        a_out.start()
        merged(0, 1024, 2048)
        b_out.start()
        polls[1]()
        compute(2, order[2])
        pair(2).start()
        pair(1).wait_recv()
        merged(1, 1024, 2048)
        r_soon.start()
        polls[2]()
        compute(3, order[3])
        pair(3).start()
        pair(2).wait_recv()
        merged(2, 0, 1024)
        l_soon.start()
        a_out.wait_recv()
        merged(1, 0, 1024, ra)
        r_late.start()
        b_out.wait_recv()
        merged(2, 1024, 2048, rb)
        l_late.start()
        polls[3]()
        pair(3).wait_recv()
        for op in (r_soon, l_soon, r_late, l_late):
            op.wait_recv()

        def drain():
            for j in range(4):
                pair(j).wait_send()
            for op in (a_out, b_out, r_late, r_soon, l_soon, l_late):
                op.wait_send()

        return drain

    def summed(s, r):
        v = part[s, 3, c, r, :].astype(F32) + d2[s, 3, r, :].astype(F32)
        return v + rl[s, r, :].astype(F32) + rr[s, r, :].astype(F32)

    def normed(v, i):
        mean = jnp.mean(v, axis=-1, keepdims=True)
        v = v - mean
        var = jnp.mean(v * v, axis=-1, keepdims=True)
        return v * lax.rsqrt(var + EPS) * gain_ref[i : i + 1, :] + bias_ref[i : i + 1, :]

    for i in (8, 9):
        loads[i].wait()

    def attend(j, b):
        rows = pl.ds(pl.multiple_of(b * BLK, BLK), BLK)
        state = dpre[b][0:1, 0:1] * inc[...].reshape(BLK, 512).astype(F32) + loc[b]
        mixed = within[b] + jnp.dot(sq[b], state.astype(BF16), preferred_element_type=F32)
        mean = jnp.mean(mixed, axis=-1, keepdims=True)
        mixed = mixed - mean
        var = jnp.mean(mixed * mixed, axis=-1, keepdims=True)
        mixed = mixed * lax.rsqrt(var + EPS)
        gate = gv[rows, :].astype(F32)
        gr[...] = (gate * jax.nn.sigmoid(gate) * mixed).astype(BF16)

        def tile(n, carry):
            cols = pl.ds(pl.multiple_of(n * 512, 512), 512)
            p = jnp.dot(gr[...], owv[:, cols], preferred_element_type=F32)
            part[0, j, :, :, cols] = p.astype(BF16).reshape(2, 128, 512)
            return carry

        lax.fori_loop(0, 4, tile, 0)

    def poll_w(*fs):
        def run():
            for f in fs:
                f()

        return run

    loads[4].wait()
    drain0 = reduce_scatter(
        0,
        attend,
        (
            poll_w(functools.partial(u3, 1)),
            poll_w(functools.partial(u3, 2)),
            poll_w(functools.partial(u3, 3), n0, n0b),
            poll_w(u4, n1),
        ),
    )
    loads[10].wait()

    def first_norm(i, carry):
        r = pl.ds(pl.multiple_of(i * 16, 16), 16)
        v = ALPHA * rv[r, :].astype(F32) + summed(0, r)
        xb[t, r, :] = normed(v, 0).astype(BF16)
        return carry

    lax.fori_loop(0, 8, first_norm, 0)

    tl, tr, to = xl * 2 + c, xr * 2 + c, xo * 2 + c
    R0, R1, RA = slice(0, 64), slice(64, 128), slice(0, 128)

    def ag(n, dev_t, rows, dev):
        p = xb.at[dev_t, rows, :]
        return remote(p, p, ag_s.at[n], ag_r.at[n], dev)

    sends = []

    def go(n, dev_t, rows, dev):
        op = ag(n, dev_t, rows, dev)
        op.start()
        sends.append(op)

    def arrived(n, dev_t, rows):
        ag(n, dev_t, rows, SIB).wait_recv()

    go(1, t, R0, XR)
    go(3, t, R1, XL)
    go(0, t, RA, SIB)
    go(2, t, R1, XR)
    go(4, t, R0, XL)

    def up(b):
        rows = pl.ds(pl.multiple_of(16 + b * BLK, 16), BLK)

        def tile(n, carry):
            cols = pl.ds(pl.multiple_of(n * 256, 256), 256)
            lhs = xb[pl.ds(2 * b, 2)].reshape(BLK, 2048)
            w = wu[:, :, cols].reshape(2048, 256)
            ub[rows, cols] = jnp.dot(lhs, w, preferred_element_type=F32).astype(BF16)
            return carry

        lax.fori_loop(0, 5, tile, 0)
        lhs = xb[pl.ds(2 * b, 2)].reshape(BLK, 2048)
        w = wu[:, :, 1280:1408].reshape(2048, 128)
        ub[rows, 1280:1408] = jnp.dot(lhs, w, preferred_element_type=F32).astype(BF16)

    def halo_copy():
        nxt = lax.rem(me + 1, NSP)
        dev = {"z": lax.div(nxt, 4), "y": lax.rem(nxt, 4)}
        return remote(ub.at[1024:1040, :], halo, h_s.at[0], h_r.at[0], dev)

    def send_halo(when):
        @pl.when(jnp.logical_and(when, me < NSP - 1))
        def _():
            halo_copy().start()

    def take_halo(when):
        @pl.when(jnp.logical_and(when, me > 0))
        def _():
            halo_copy().wait_recv()
            ub[0:16, :] = halo[...]

    @pl.when(me == 0)
    def _():
        ub[0:16, :] = jnp.zeros((16, 1408), BF16)

    def conv(b):
        def three(block, half, n):
            w = taps_ref[3 * half : 3 * half + 3, n * 128 : (n + 1) * 128]
            shift = taps_ref[6 + half : 7 + half, n * 128 : (n + 1) * 128]
            v = shift + block[14:270] * w[0:1]
            v = v + block[15:271] * w[1:2]
            return v + block[16:272] * w[2:3]

        rows = pl.ds(pl.multiple_of(b * BLK, BLK), BLK)
        around = pl.ds(pl.multiple_of(b * BLK, BLK), BLK + 16)
        for n in range(6):
            if n < 5:
                g = ub[around, n * 128 : (n + 1) * 128].astype(F32)
                v = ub[around, 640 + n * 128 : 640 + (n + 1) * 128].astype(F32)
            else:
                g = ub[around, 1280:1408].astype(F32)
                v = pltpu.roll(g, 64, 1)
            a = jax.nn.gelu(three(g, 0, n)) * three(v, 1, n)
            if n == 5:
                lane = lax.broadcasted_iota(jnp.int32, (BLK, 128), 1)
                a = jnp.where(lane < 64, a, 0.0)
            act[rows, n * 128 : (n + 1) * 128] = a.astype(BF16)

    arrived(0, t + 1 - 2 * c, RA)
    n2()
    up(x)
    send_halo(x == 3)
    arrived(1, tl, R0)
    go(5, tl, R0, XR)
    arrived(3, tr, R1)
    go(6, tr, R1, XL)
    go(7, tl, R0, SIB)
    go(8, tr, R1, SIB)
    n3(0)
    n3(1)
    arrived(2, tl, R1)
    go(9, tl, R1, SIB)
    arrived(4, tr, R0)
    go(10, tr, R0, SIB)
    n3(2)
    n3(3)
    arrived(7, xl * 2 + 1 - c, R0)
    arrived(8, xr * 2 + 1 - c, R1)
    arrived(9, xl * 2 + 1 - c, R1)
    arrived(10, xr * 2 + 1 - c, R0)
    up(xr)
    send_halo(xr == 3)
    up(xl)
    send_halo(xl == 3)
    arrived(5, to, R0)
    go(11, to, R0, SIB)
    arrived(6, to, R1)
    go(12, to, R1, SIB)
    take_halo(x == 3)
    conv(xr)
    arrived(11, xo * 2 + 1 - c, R0)
    arrived(12, xo * 2 + 1 - c, R1)
    up(xo)
    send_halo(xo == 3)
    take_halo(x == 2)
    conv(xo)
    n4()

    def down(j, b):
        if j == 2:
            take_halo(x == 1)
            conv(xl)
        if j == 3:
            take_halo(x == 0)
            conv(x)
        rows = pl.ds(pl.multiple_of(b * BLK, BLK), BLK)

        def tile(n, carry):
            cols = pl.ds(pl.multiple_of(n * 512, 512), 512)
            p = jnp.dot(act[rows, :], wd[:, cols], preferred_element_type=F32)
            part[1, j, :, :, cols] = p.astype(BF16).reshape(2, 128, 512)
            return carry

        lax.fori_loop(0, 4, tile, 0)

    def nothing():
        pass

    drain1 = reduce_scatter(1, down, (nothing,) * 4)

    def last_norm(i, carry):
        r = pl.ds(pl.multiple_of(i * 16, 16), 16)
        v = ALPHA * xb[t, r, :].astype(F32) + summed(1, r)
        o_ref[r, :] = normed(v, 1).astype(BF16)
        return carry

    lax.fori_loop(0, 8, last_norm, 0)

    def drain_state(i, carry):
        j, dev = sp_peer(i)
        remote(ssend.at[j], srecv.at[me], ss_s.at[j], ss_r.at[me], dev).wait_send()
        remote(rsend.at[j], inc.at[me], rs_s.at[j], rs_r.at[me], dev).wait_send()
        return carry

    lax.fori_loop(1, NSP, drain_state, 0)
    udrain()
    ndrain()
    drain0()
    drain1()
    for op in sends:
        op.wait_send()

    @pl.when(me < NSP - 1)
    def _():
        halo_copy().wait_send()


def shards(q, k, v, g, logd, res, ow, gain, bias, ug, uv, cw, cbias, dw):
    ti, tb = position_tables()
    taps = jnp.concatenate([cw.reshape(6, FF), cbias], axis=0)
    taps = jnp.pad(taps, ((0, 0), (0, FFP - FF)))
    dma = pltpu.SemaphoreType.DMA
    vm = pl.BlockSpec(memory_space=pltpu.VMEM)
    hb = pl.BlockSpec(memory_space=pl.ANY)
    return pl.pallas_call(
        body,
        out_shape=jax.ShapeDtypeStruct((128, 2048), BF16),
        in_specs=[hb, hb, hb, hb, vm, hb, hb, vm, vm, hb, hb, vm, hb, vm, vm],
        out_specs=vm,
        scratch_shapes=[
            pltpu.VMEM((1024, 256), BF16),
            pltpu.VMEM((1024, 256), BF16),
            pltpu.VMEM((1024, 512), BF16),
            pltpu.VMEM((1024, 512), BF16),
            pltpu.VMEM((128, 2048), BF16),
            pltpu.VMEM((512, 2048), BF16),
            pltpu.VMEM((1408, 128), BF16),
            pltpu.VMEM((NSP, 128, 1408), BF16),
            pltpu.VMEM((FFP, 2048), BF16),
            pltpu.VMEM((8, 256), F32),
            pltpu.VMEM((8, 256), F32),
            pltpu.VMEM((256, 8), F32),
            pltpu.VMEM((4, 8, 128), F32),
            pltpu.VMEM((4, 256, 256), BF16),
            pltpu.VMEM((4, 256, 256), BF16),
            pltpu.VMEM((5, 256, 512), F32),
            pltpu.VMEM((4, 256, 512), F32),
            pltpu.VMEM((256, 512), BF16),
            pltpu.VMEM((NSP, 16, 640), BF16),
            pltpu.VMEM((NSP, 16, 640), BF16),
            pltpu.VMEM((NSP, 16, 512), BF16),
            pltpu.VMEM((NSP, 16, 512), BF16),
            pltpu.VMEM((2, 4, 2, 128, 2048), BF16),
            pltpu.VMEM((2, 4, 128, 2048), BF16),
            pltpu.VMEM((2, 3, 128, 2048), BF16),
            pltpu.VMEM((2, 128, 1024), BF16),
            pltpu.VMEM((2, 128, 1024), BF16),
            pltpu.VMEM((2, 128, 2048), BF16),
            pltpu.VMEM((2, 128, 2048), BF16),
            pltpu.VMEM((8, 128, 2048), BF16),
            pltpu.VMEM((1040, 1408), BF16),
            pltpu.VMEM((1024, FFP), BF16),
            pltpu.VMEM((16, 1408), BF16),
            dma((11,)),
            dma((NSP,)),
            dma((NSP,)),
            dma((NSP,)),
            dma((NSP,)),
            dma((2, 40)),
            dma((2, 40)),
            dma((2, 4)),
            dma((2, 4)),
            dma((2, 6)),
            dma((2, 6)),
            dma((13,)),
            dma((13,)),
            dma((1,)),
            dma((1,)),
        ],
        compiler_params=pltpu.CompilerParams(
            collective_id=0, has_side_effects=True, vmem_limit_bytes=62 * 1024 * 1024
        ),
        name="layer",
    )(q, k, v, g, logd.reshape(8, 128), res, ow, gain, bias, ug.T, uv.T, taps, dw, ti, tb)


def solution(mesh):
    torus = Mesh(mesh.devices.reshape(4, 4, 4, 2), ("z", "y", "x", "c"))
    sp, tp = ("z", "y"), ("x", "c")
    return jax.shard_map(
        shards,
        mesh=torus,
        in_specs=(
            P(sp, tp),
            P(sp, tp),
            P(sp, tp),
            P(sp, tp),
            P(sp, tp),
            P(sp, None),
            P(tp, None),
            P(),
            P(),
            P(sp, tp),
            P(sp, tp),
            P(None, None, tp),
            P(None, tp),
            P(tp, sp),
        ),
        out_specs=P(sp + tp, None),
        check_vma=False,
    )
```

time: 289 us -> 121 us (0.42)
  waiting for transfers between devices: 129 us -> 0 us
  Pallas kernels: 0 us -> 116 us
  other arithmetic: 58.1 us -> 1.31 us
  matrix products: 39.6 us -> 0 us
  between operations: 20.6 us -> 0.01 us
  blocking collectives: 18.5 us -> 0 us
  local copies, waits for them, and re-layouts: 13.1 us -> 2.63 us
  starting transfers between devices: 6.72 us -> 0 us
    pallas_call x0 -> x1, Pallas kernels: none -> 116 us  [shards(): pl.pallas_call(body, out_shape=jax.ShapeDtypeStruct((128, 2048), BF16), i...]
    psum x1 -> x0, waiting for transfers between devices: 71.7 us -> none  [shards(): lax.psum(partial_rows.astype(jnp.bfloat16), 'tp').astype(jnp.float32)]
    dot_general x10 -> x0, matrix products: 39.6 us -> none  [the longest x1 9.97 us: shards(): jnp.dot(activated, full_down, preferred_element_type=jnp.float32)]
    reduce_scatter x1 -> x0, waiting for transfers between devices: 38.4 us -> none  [shards(): lax.psum_scatter(partial_ffn.astype(jnp.bfloat16), 'tp', scatter_dimensio...]
    add x9 -> x0, other arithmetic: 18.8 us -> none  [the longest x4 7.52 us: advance(): return (pieces[2][:, None, None] * carry_state + pieces[1], carried)]
    unnamed x2 -> x0, blocking collectives: 18.5 us -> none
    all_gather x3 -> x0, waiting for transfers between devices: 17.2 us -> none  [the longest x2 17.1 us: entering(): lax.all_gather(part.astype(kind), axis)]
    convert_element_type x10 -> x0, other arithmetic: 16.1 us -> none  [the longest x3 5.34 us: entering(): part.astype(kind)]
  transfers between devices with their start and end apart: 7 -> 0, of which waited for: 5 -> 0; matrix products, arithmetic and copies ran while one was open for 10% -> 0% of each run, Pallas kernels for 0% -> 0%
where the time goes in v1:
time: 121 us; the launch traced here: 120 us
  Pallas kernels  116 us (96%)
  local copies, waits for them, and re-layouts  2.63 us (2%)
  other arithmetic  1.31 us (1%)
    pallas_call x1, Pallas kernels, shards(): pl.pallas_call(body, out_shape=jax.ShapeDtypeStruct((128, 2048), BF16), i...  116 us
    unnamed x2, local copies, waits for them, and re-layouts  2.61 us

profile of v1, /device:TPU:1, one launch (start us, length us, event | category | flops | bytes accessed | tf_op | source)
XLA Modules:
  0.0 120.3 jit_solution(12630757374592977320)
XLA Ops:
  0.0 0.7 copy.18
  0.7 1.3 %select_maximum_fusion.taps_ref = f32[8,768]{1,0:T(8,128)} fusion(f32[2,704]{1,0:T(2,128)} %param.28, f32[6,704]{1,0:T(8,128)S(1)} %reshape.7), kind=kLoop, calls=%fused_computation | loop fusion | flops 24576 | bytes 47104 | tf_op jit(solution)/shard_map/concatenate | solution.py:619
  2.1 116.4 %layer.1 = bf16[128,2048]{1,0:T(8,128)(2,1)} custom-call(bf16[1024,256]{1,0:T(8,128)(2,1)} %q_h.1, bf16[1024,256]{1,0:T(8,128)(2,1)} %k_h.1, bf16[1024,512]{1,0:T(8,128)(2,1)} %v_h.1, bf16[1024,512]{1,0:T(8,128)(2,1)} %g_h.1, f32[8,128]{1,0:T(8,128)} %bitcast.5, bf16[1024,2048]{1,0:T(8,128)(2,1)} %res_h.1, bf16[512,2048]{1,0:T(8,128)(2,1)} %ow_h.1, ...), custom_call_target="tpu_custom_call" | custom-call | tf_op jit(solution)/shard_map/layer/pallas_call | solution.py:624
  118.5 1.9 %copy.20 = bf16[128,2048]{1,0:T(8,128)(2,1)} copy(bf16[128,2048]{1,0:T(8,128)(2,1)} %layer.1) | data formatting | bytes 1048576
  (1 shorter events, 0.0 us)

commit v2 on v1

--- a/solution.py
+++ b/solution.py
@@ -35,9 +35,10 @@
 
 
 def body(
-    q_h, k_h, v_h, g_h, log_ref, res_h, ow_h, gain_ref, bias_ref, ug_h, uv_h, taps_ref, dw_h,
-    ti_ref, tb_ref, o_ref,
-    qv, kv, vv, gv, rv, owv, ust, wu, wd,
+    q_h, k_h, v_h, g_h, log_h, res_h, ow_h, gain_h, bias_h, ug_h, uv_h, taps_h, shift_h, dw_h,
+    ti_h, tb_h, o_ref,
+    qv, kv, vv, gv, log_ref, rv, owv, gain_ref, bias_ref, ust, taps_ref, shift_ref, ti_ref, tb_ref,
+    wu, wd,
     lsc, crow, ccol, dpre, kr, sq, loc, within, gr,
     ssend, srecv, rsend, inc,
     part, d2, cb, ra, rb, rl, rr,
@@ -61,22 +62,36 @@
             device_id_type=MESH,
         )
 
-    loads = [
-        (ug_h.at[0:640], ust.at[0:640]),
-        (uv_h.at[0:640], ust.at[640:1280]),
-        (ug_h.at[640:704], ust.at[1280:1344]),
-        (uv_h.at[640:704], ust.at[1344:1408]),
-        (dw_h, wd.at[0:FF, pl.ds(pl.multiple_of(me * 128, 128), 128)]),
-        (k_h, kv),
-        (v_h, vv),
-        (q_h, qv),
-        (g_h, gv),
-        (ow_h, owv),
-        (res_h.at[pl.ds(pl.multiple_of(t * 128, 128), 128)], rv),
-    ]
-    loads = [pltpu.make_async_copy(s, d, in_sem.at[i]) for i, (s, d) in enumerate(loads)]
-    for load in loads:
+    loads = {
+        "log": (log_h, log_ref),
+        "k": (k_h, kv),
+        "ti": (ti_h, ti_ref),
+        "tb": (tb_h.at[me], tb_ref),
+        "v": (v_h, vv),
+        "ug": (ug_h.at[0:640], ust.at[0:640]),
+        "uv": (uv_h.at[0:640], ust.at[640:1280]),
+        "ug2": (ug_h.at[640:704], ust.at[1280:1344]),
+        "uv2": (uv_h.at[640:704], ust.at[1344:1408]),
+        "q": (q_h, qv),
+        "g": (g_h, gv),
+        "ow": (ow_h, owv),
+        "dw": (dw_h, wd.at[0:FF, pl.ds(pl.multiple_of(me * 128, 128), 128)]),
+        "res": (res_h.at[pl.ds(pl.multiple_of(t * 128, 128), 128)], rv),
+        "gain": (gain_h, gain_ref),
+        "bias": (bias_h, bias_ref),
+        "taps": (taps_h, taps_ref),
+        "shift": (shift_h, shift_ref),
+    }
+    loads = {
+        name: pltpu.make_async_copy(src, dst, in_sem.at[i])
+        for i, (name, (src, dst)) in enumerate(loads.items())
+    }
+    for load in loads.values():
         load.start()
+
+    def loaded(*names):
+        for name in names:
+            loads[name].wait()
 
     barrier = pltpu.get_barrier_semaphore()
 
@@ -187,30 +202,20 @@
     u0, u0b, u1, u2, u3, u4, udrain = gather(0, up_piece)
     n0, n0b, n1, n2, n3, n4, ndrain = gather(1, dn_piece)
 
-    lsc[...] = jnp.zeros((8, 256), F32)
-    for b in range(4):
-        lsc[b : b + 1, 0:128] = log_ref[2 * b : 2 * b + 1, :]
-        lsc[b : b + 1, 128:256] = log_ref[2 * b + 1 : 2 * b + 2, :]
     ri = lax.broadcasted_iota(jnp.int32, (BLK, BLK), 0)
     ci = lax.broadcasted_iota(jnp.int32, (BLK, BLK), 1)
     causal = ri >= ci
     tri = jnp.where(causal, 1.0, 0.0).astype(F32)
+    lsc[...] = jnp.zeros((8, 256), F32)
+    loaded("log")
+    for b in range(4):
+        lsc[b : b + 1, 0:128] = log_ref[2 * b : 2 * b + 1, :]
+        lsc[b : b + 1, 128:256] = log_ref[2 * b + 1 : 2 * b + 2, :]
     logs = lsc[...]
     crow[...] = lax.dot_general(logs, tri, NT, precision=HIGH, preferred_element_type=F32)
     ccol[...] = lax.dot_general(tri, logs, NT, precision=HIGH, preferred_element_type=F32)
-
-    wd[FF:FFP, :] = jnp.zeros((FFP - FF, 2048), BF16)
-
-    for i in range(4):
-        loads[i].wait()
-    for n in range(11):
-        tile = ust[n * 128 : (n + 1) * 128, :].astype(F32)
-        wu[me, :, n * 128 : (n + 1) * 128] = tile.T.astype(BF16)
-    pl.semaphore_wait(barrier, NSP + 2)
-    u0()
-    u0b()
-
-    base = tb_ref[me]
+    loaded("k", "ti", "tb", "v")
+    base = tb_ref[...]
 
     def turned(ref, b):
         ci_, si_ = ti_ref[0], ti_ref[1]
@@ -221,8 +226,6 @@
         second = ref[b * BLK : (b + 1) * BLK, 128:256].astype(F32)
         return front * cos - second * sin, front * sin + second * cos
 
-    loads[5].wait()
-    loads[6].wait()
     decay = jnp.ones((1, 1), F32)
     for b in range(4):
         front, second = turned(kv, b)
@@ -257,7 +260,8 @@
     for j in range(NSP):
         ssend[j, :, 0:512] = loc[4, j * 16 : (j + 1) * 16, :].astype(BF16)
         ssend[j, :, 512:640] = tag
-    srecv[me] = ssend[me]
+
+    pl.semaphore_wait(barrier, NSP + 2)
 
     def scatter(i, carry):
         j, dev = sp_peer(i)
@@ -265,9 +269,15 @@
         return carry
 
     lax.fori_loop(1, NSP, scatter, 0)
-    u1()
-
-    loads[7].wait()
+    srecv[me] = ssend[me]
+
+    loaded("ug", "uv", "ug2", "uv2")
+    for n in range(11):
+        tile = ust[n * 128 : (n + 1) * 128, :].astype(F32)
+        wu[me, :, n * 128 : (n + 1) * 128] = tile.T.astype(BF16)
+    u0()
+
+    loaded("q")
     for b in range(4):
         front, second = turned(qv, b)
         qr = jnp.concatenate([front, second], axis=1).astype(BF16)
@@ -281,6 +291,8 @@
             vv[b * BLK : (b + 1) * BLK, :],
             preferred_element_type=F32,
         )
+    wd[FF:FFP, :] = jnp.zeros((FFP - FF, 2048), BF16)
+    act[:, FF:FFP] = jnp.zeros((1024, FFP - FF), BF16)
 
     def scattered(i, carry):
         j, dev = sp_peer(i)
@@ -303,8 +315,8 @@
         return carry
 
     lax.fori_loop(1, NSP, give_back, 0)
-    u2()
-    u3(0)
+    u0b()
+    u1()
 
     def given(i, carry):
         j, dev = sp_peer(i)
@@ -345,7 +357,6 @@
 
         compute(0, order[0])
         pair(0).start()
-        polls[0]()
         compute(1, order[1])
         pair(1).start()
         pair(0).wait_recv()
@@ -353,25 +364,24 @@
         a_out.start()
         merged(0, 1024, 2048)
         b_out.start()
-        polls[1]()
         compute(2, order[2])
         pair(2).start()
         pair(1).wait_recv()
         merged(1, 1024, 2048)
         r_soon.start()
-        polls[2]()
         compute(3, order[3])
         pair(3).start()
         pair(2).wait_recv()
         merged(2, 0, 1024)
         l_soon.start()
+        polls[0]()
         a_out.wait_recv()
         merged(1, 0, 1024, ra)
         r_late.start()
         b_out.wait_recv()
         merged(2, 1024, 2048, rb)
         l_late.start()
-        polls[3]()
+        polls[1]()
         pair(3).wait_recv()
         for op in (r_soon, l_soon, r_late, l_late):
             op.wait_recv()
@@ -394,8 +404,7 @@
         var = jnp.mean(v * v, axis=-1, keepdims=True)
         return v * lax.rsqrt(var + EPS) * gain_ref[i : i + 1, :] + bias_ref[i : i + 1, :]
 
-    for i in (8, 9):
-        loads[i].wait()
+    loaded("g", "ow")
 
     def attend(j, b):
         rows = pl.ds(pl.multiple_of(b * BLK, BLK), BLK)
@@ -416,33 +425,26 @@
 
         lax.fori_loop(0, 4, tile, 0)
 
-    def poll_w(*fs):
-        def run():
-            for f in fs:
-                f()
-
-        return run
-
-    loads[4].wait()
-    drain0 = reduce_scatter(
-        0,
-        attend,
-        (
-            poll_w(functools.partial(u3, 1)),
-            poll_w(functools.partial(u3, 2)),
-            poll_w(functools.partial(u3, 3), n0, n0b),
-            poll_w(u4, n1),
-        ),
-    )
-    loads[10].wait()
+    def early():
+        u2()
+        u3(0)
+        u3(1)
+
+    def later():
+        u3(2)
+        u3(3)
+        loaded("dw")
+        n0()
+        n0b()
+
+    drain0 = reduce_scatter(0, attend, (early, later))
+    loaded("res", "gain", "bias")
 
     def first_norm(i, carry):
-        r = pl.ds(pl.multiple_of(i * 16, 16), 16)
+        r = pl.ds(pl.multiple_of(i * 32, 32), 32)
         v = ALPHA * rv[r, :].astype(F32) + summed(0, r)
         xb[t, r, :] = normed(v, 0).astype(BF16)
         return carry
-
-    lax.fori_loop(0, 8, first_norm, 0)
 
     tl, tr, to = xl * 2 + c, xr * 2 + c, xo * 2 + c
     R0, R1, RA = slice(0, 64), slice(64, 128), slice(0, 128)
@@ -461,7 +463,9 @@
     def arrived(n, dev_t, rows):
         ag(n, dev_t, rows, SIB).wait_recv()
 
+    lax.fori_loop(0, 2, first_norm, 0)
     go(1, t, R0, XR)
+    lax.fori_loop(2, 4, first_norm, 0)
     go(3, t, R1, XL)
     go(0, t, RA, SIB)
     go(2, t, R1, XR)
@@ -503,30 +507,29 @@
         ub[0:16, :] = jnp.zeros((16, 1408), BF16)
 
     def conv(b):
-        def three(block, half, n):
-            w = taps_ref[3 * half : 3 * half + 3, n * 128 : (n + 1) * 128]
-            shift = taps_ref[6 + half : 7 + half, n * 128 : (n + 1) * 128]
-            v = shift + block[14:270] * w[0:1]
-            v = v + block[15:271] * w[1:2]
-            return v + block[16:272] * w[2:3]
+        def three(block, half, lanes):
+            v = shift_ref[half : half + 1, lanes] + block[14:270] * taps_ref[0, half : half + 1, lanes]
+            v = v + block[15:271] * taps_ref[1, half : half + 1, lanes]
+            return v + block[16:272] * taps_ref[2, half : half + 1, lanes]
 
         rows = pl.ds(pl.multiple_of(b * BLK, BLK), BLK)
         around = pl.ds(pl.multiple_of(b * BLK, BLK), BLK + 16)
         for n in range(6):
             if n < 5:
-                g = ub[around, n * 128 : (n + 1) * 128].astype(F32)
+                lanes = slice(n * 128, (n + 1) * 128)
+                g = ub[around, lanes].astype(F32)
                 v = ub[around, 640 + n * 128 : 640 + (n + 1) * 128].astype(F32)
             else:
-                g = ub[around, 1280:1408].astype(F32)
-                v = pltpu.roll(g, 64, 1)
-            a = jax.nn.gelu(three(g, 0, n)) * three(v, 1, n)
-            if n == 5:
-                lane = lax.broadcasted_iota(jnp.int32, (BLK, 128), 1)
-                a = jnp.where(lane < 64, a, 0.0)
-            act[rows, n * 128 : (n + 1) * 128] = a.astype(BF16)
+                lanes = slice(640, FF)
+                both = ub[around, 1280:1408].astype(F32)
+                g, v = both[:, 0:64], pltpu.roll(both, 64, 1)[:, 0:64]
+            a = jax.nn.gelu(three(g, 0, lanes)) * three(v, 1, lanes)
+            act[rows, lanes] = a.astype(BF16)
 
     arrived(0, t + 1 - 2 * c, RA)
-    n2()
+    u4()
+    n1()
+    loaded("taps", "shift")
     up(x)
     send_halo(x == 3)
     arrived(1, tl, R0)
@@ -535,6 +538,7 @@
     go(6, tr, R1, XL)
     go(7, tl, R0, SIB)
     go(8, tr, R1, SIB)
+    n2()
     n3(0)
     n3(1)
     arrived(2, tl, R1)
@@ -585,15 +589,15 @@
     def nothing():
         pass
 
-    drain1 = reduce_scatter(1, down, (nothing,) * 4)
+    drain1 = reduce_scatter(1, down, (nothing, nothing))
 
     def last_norm(i, carry):
-        r = pl.ds(pl.multiple_of(i * 16, 16), 16)
+        r = pl.ds(pl.multiple_of(i * 32, 32), 32)
         v = ALPHA * xb[t, r, :].astype(F32) + summed(1, r)
         o_ref[r, :] = normed(v, 1).astype(BF16)
         return carry
 
-    lax.fori_loop(0, 8, last_norm, 0)
+    lax.fori_loop(0, 4, last_norm, 0)
 
     def drain_state(i, carry):
         j, dev = sp_peer(i)
@@ -616,24 +620,29 @@
 
 def shards(q, k, v, g, logd, res, ow, gain, bias, ug, uv, cw, cbias, dw):
     ti, tb = position_tables()
-    taps = jnp.concatenate([cw.reshape(6, FF), cbias], axis=0)
-    taps = jnp.pad(taps, ((0, 0), (0, FFP - FF)))
     dma = pltpu.SemaphoreType.DMA
     vm = pl.BlockSpec(memory_space=pltpu.VMEM)
     hb = pl.BlockSpec(memory_space=pl.ANY)
     return pl.pallas_call(
         body,
         out_shape=jax.ShapeDtypeStruct((128, 2048), BF16),
-        in_specs=[hb, hb, hb, hb, vm, hb, hb, vm, vm, hb, hb, vm, hb, vm, vm],
+        in_specs=[hb] * 16,
         out_specs=vm,
         scratch_shapes=[
             pltpu.VMEM((1024, 256), BF16),
             pltpu.VMEM((1024, 256), BF16),
             pltpu.VMEM((1024, 512), BF16),
             pltpu.VMEM((1024, 512), BF16),
+            pltpu.VMEM((8, 128), F32),
             pltpu.VMEM((128, 2048), BF16),
             pltpu.VMEM((512, 2048), BF16),
+            pltpu.VMEM((2, 2048), F32),
+            pltpu.VMEM((2, 2048), F32),
             pltpu.VMEM((1408, 128), BF16),
+            pltpu.VMEM((3, 2, FF), F32),
+            pltpu.VMEM((2, FF), F32),
+            pltpu.VMEM((2, BLK, 128), F32),
+            pltpu.VMEM((8, 128), F32),
             pltpu.VMEM((NSP, 128, 1408), BF16),
             pltpu.VMEM((FFP, 2048), BF16),
             pltpu.VMEM((8, 256), F32),
@@ -660,7 +669,7 @@
             pltpu.VMEM((1040, 1408), BF16),
             pltpu.VMEM((1024, FFP), BF16),
             pltpu.VMEM((16, 1408), BF16),
-            dma((11,)),
+            dma((18,)),
             dma((NSP,)),
             dma((NSP,)),
             dma((NSP,)),
@@ -680,7 +689,10 @@
             collective_id=0, has_side_effects=True, vmem_limit_bytes=62 * 1024 * 1024
         ),
         name="layer",
-    )(q, k, v, g, logd.reshape(8, 128), res, ow, gain, bias, ug.T, uv.T, taps, dw, ti, tb)
+    )(
+        q, k, v, g, logd.reshape(8, 128), res, ow, gain, bias, ug.T, uv.T,
+        cw.transpose(1, 0, 2), cbias, dw, ti, tb,
+    )
 
 
 def solution(mesh):

time: 121 us -> 103 us (0.85)
  Pallas kernels: 116 us -> 101 us
  other arithmetic: 1.31 us -> 0 us
    pallas_call x1, Pallas kernels: 116 us -> 101 us  [shards(): pl.pallas_call(body, out_shape=jax.ShapeDtypeStruct((128, 2048), BF16), i...]
    concatenate x1 -> x0, other arithmetic: 1.31 us -> none  [shards(): taps = jnp.concatenate([cw.reshape(6, FF), cbias], axis=0)]
    unnamed x2 -> x1, local copies, waits for them, and re-layouts: 2.61 us -> 1.88 us
where the time goes in v2:
time: 103 us
  Pallas kernels  101 us (98%)
  local copies, waits for them, and re-layouts  1.88 us (2%)
    pallas_call x1, Pallas kernels, shards(): pl.pallas_call(body, out_shape=jax.ShapeDtypeStruct((128, 2048), BF16), i...  101 us

profile of v2, /device:TPU:1, one launch (start us, length us, event | category | flops | bytes accessed | tf_op | source)
XLA Modules:
  0.0 102.7 jit_solution(757362994298359679)
XLA Ops:
  0.0 100.8 %layer.1 = bf16[128,2048]{1,0:T(8,128)(2,1)} custom-call(bf16[1024,256]{1,0:T(8,128)(2,1)} %q_h.1, bf16[1024,256]{1,0:T(8,128)(2,1)} %k_h.1, bf16[1024,512]{1,0:T(8,128)(2,1)} %v_h.1, bf16[1024,512]{1,0:T(8,128)(2,1)} %g_h.1, f32[8,128]{1,0:T(8,128)} %bitcast.7, bf16[1024,2048]{1,0:T(8,128)(2,1)} %res_h.1, bf16[512,2048]{1,0:T(8,128)(2,1)} %ow_h.1, ...), custom_call_target="tpu_custom_call" | custom-call | tf_op jit(solution)/shard_map/layer/pallas_call | solution.py:626
  100.8 1.9 %copy.18 = bf16[128,2048]{1,0:T(8,128)(2,1)} copy(bf16[128,2048]{1,0:T(8,128)(2,1)} %layer.1) | data formatting | bytes 1048576

commit v3 on v2

v3 whole, which is shorter than its diff:
```python
import functools

import jax
import jax.numpy as jnp
import numpy as np
from jax import lax
from jax.experimental import pallas as pl
from jax.experimental.pallas import tpu as pltpu
from jax.sharding import Mesh
from jax.sharding import PartitionSpec as P

F32 = jnp.float32
BF16 = jnp.bfloat16
HIGH = lax.Precision.HIGHEST
MESH = pl.DeviceIdType.MESH
ALPHA = 8.0**0.25
EPS = 1e-05
NSP = 16
BLK = 256
FF = 704
FFP = 768
ROWS = (((64, 128), (0, 64)), ((80, 128), (0, 80)))
NT = (((1,), (1,)), ((), ()))
TN = (((0,), (0,)), ((), ()))


def position_tables():
    freq = 10000.0 ** (-2.0 * np.arange(128, dtype=np.float64) / 256.0)
    inner = np.arange(BLK, dtype=np.float64)[:, None] * freq[None]
    start = np.arange(4 * NSP, dtype=np.float64)[:, None] * BLK * freq[None]
    ti = np.stack([np.cos(inner), np.sin(inner)]).astype(np.float32)
    tb = np.concatenate(
        [np.cos(start).reshape(NSP, 4, 128), np.sin(start).reshape(NSP, 4, 128)], axis=1
    ).astype(np.float32)
    return ti, tb


def body(
    q_h, k_h, v_h, g_h, log_h, res_h, ow_h, gain_h, bias_h, ug_h, uv_h, taps_h, shift_h, dw_h,
    ti_h, tb_h, o_ref,
    qv, kv, vv, gv, log_ref, rv, owv, gain_ref, bias_ref, ust, taps_ref, shift_ref, ti_ref, tb_ref,
    wu, wd,
    lsc, crow, ccol, dpre, kr, sq, loc, within, gr,
    ssend, srecv, rsend, inc,
    part, d2, cb, ra, rb, rl, rr,
    xb, ub, act0, act1, halo, ov,
    in_sem, st_s, st_r, wg_s, wg_r, d2_s, d2_r, x_s, x_r, ag_s, ag_r, h_s, h_r, out_sem,
):
    z, y, x, c = (lax.axis_index(a) for a in ("z", "y", "x", "c"))
    me = z * 4 + y
    t = x * 2 + c
    xr, xl, xo = lax.rem(x + 1, 4), lax.rem(x + 3, 4), lax.rem(x + 2, 4)

    def at(axis, value):
        return {axis: value}

    SIB = at("c", 1 - c)
    XR, XL = at("x", xr), at("x", xl)

    def remote(src, dst, ssem, rsem, dev):
        return pltpu.make_async_remote_copy(
            src_ref=src, dst_ref=dst, send_sem=ssem, recv_sem=rsem, device_id=dev,
            device_id_type=MESH,
        )

    loads = {
        "log": (log_h, log_ref),
        "k": (k_h, kv),
        "ti": (ti_h, ti_ref),
        "tb": (tb_h.at[me], tb_ref),
        "v": (v_h, vv),
        "ug": (ug_h.at[0:640], ust.at[0:640]),
        "uv": (uv_h.at[0:640], ust.at[640:1280]),
        "ug2": (ug_h.at[640:704], ust.at[1280:1344]),
        "uv2": (uv_h.at[640:704], ust.at[1344:1408]),
        "q": (q_h, qv),
        "g": (g_h, gv),
        "ow": (ow_h, owv),
        "dw": (dw_h, wd.at[0:FF, pl.ds(pl.multiple_of(me * 128, 128), 128)]),
        "res": (res_h.at[pl.ds(pl.multiple_of(t * 128, 128), 128)], rv),
        "gain": (gain_h, gain_ref),
        "bias": (bias_h, bias_ref),
        "taps": (taps_h, taps_ref),
        "shift": (shift_h, shift_ref),
    }
    loads = {
        name: pltpu.make_async_copy(src, dst, in_sem.at[5 if i in (6, 7, 8) else i])
        for i, (name, (src, dst)) in enumerate(loads.items())
    }
    for load in loads.values():
        load.start()

    def loaded(*names):
        for name in names:
            loads[name].wait()

    barrier = pltpu.get_barrier_semaphore()

    def sp_peer(i):
        j = lax.rem(me + i, NSP)
        return j, {"z": lax.div(j, 4), "y": lax.rem(j, 4)}

    def greet(i, carry):
        _, dev = sp_peer(i)
        pl.semaphore_signal(barrier, inc=1, device_id=dev, device_id_type=MESH)
        return carry

    lax.fori_loop(1, NSP, greet, 0)
    for dev in (SIB, XR, XL):
        pl.semaphore_signal(barrier, inc=1, device_id=dev, device_id_type=MESH)

    yr, yl, yo = lax.rem(y + 1, 4), lax.rem(y + 3, 4), lax.rem(y + 2, 4)
    zr, zl, zo = lax.rem(z + 1, 4), lax.rem(z + 3, 4), lax.rem(z + 2, 4)
    YR, YL, ZR, ZL = at("y", yr), at("y", yl), at("z", zr), at("z", zl)

    def up_piece(zz, yy, lo, n):
        return wu.at[zz * 4 + yy, lo * 16 : (lo + n) * 16, :]

    def dn_piece(zz, yy, lo, n):
        col = pl.multiple_of((zz * 4 + yy) * 128, 128)
        return wd.at[lo * 88 : (lo + n) * 88, pl.ds(col, 128)]

    def gather(g, piece, bytes_of):
        def put(n, zz, yy, lo, cnt, dev):
            p = piece(zz, yy, lo, cnt)
            remote(p, p, wg_s.at[g], wg_r.at[g, n], dev).start()

        def got(n, shards):
            p = bytes_of(shards)
            remote(p, p, wg_s.at[g], wg_r.at[g, n], YR).wait_recv()

        def s0():
            put(0, z, y, 0, 4, YR)
            put(0, z, y, 0, 4, YL)
            put(0, z, y, 4, 4, ZR)
            put(0, z, y, 4, 4, ZL)

        def s0b():
            put(2, z, y, 0, 4, ZR)
            put(2, z, y, 0, 4, ZL)
            put(2, z, y, 4, 4, YR)
            put(2, z, y, 4, 4, YL)

        def s1():
            got(0, 2)
            put(1, z, yl, 0, 2, YR)
            put(1, z, yr, 2, 2, YL)
            put(1, zl, y, 4, 2, ZR)
            put(1, zr, y, 6, 2, ZL)
            put(3, z, yl, 0, 4, ZR)
            put(3, z, yl, 0, 4, ZL)
            put(3, zl, y, 4, 4, YR)
            put(3, zl, y, 4, 4, YL)
            put(4, z, yr, 0, 4, ZR)
            put(4, z, yr, 0, 4, ZL)
            put(4, zr, y, 4, 4, YR)
            put(4, zr, y, 4, 4, YL)

        def s2():
            got(1, 1)
            put(5, z, yo, 0, 4, ZR)
            put(5, z, yo, 0, 4, ZL)
            put(5, zo, y, 4, 4, YR)
            put(5, zo, y, 4, 4, YL)

        def s3(m):
            ym, zm = (y, yl, yr, yo)[m], (z, zl, zr, zo)[m]
            got(2 + m, 2)
            put(6, zl, ym, 0, 2, ZR)
            put(6, zr, ym, 2, 2, ZL)
            put(6, zm, yl, 4, 2, YR)
            put(6, zm, yr, 6, 2, YL)

        def s4():
            got(6, 4)

        def drain():
            p = bytes_of(15)
            remote(p, p, wg_s.at[g], wg_r.at[g, 0], YR).wait_send()

        return s0, s0b, s1, s2, s3, s4, drain

    u0, u0b, u1, u2, u3, u4, udrain = gather(0, up_piece, lambda n: wu.at[0:n])
    n0, n0b, n1, n2, n3, n4, ndrain = gather(1, dn_piece, lambda n: wd.at[0:FF, 0 : n * 128])

    ri = lax.broadcasted_iota(jnp.int32, (BLK, BLK), 0)
    ci = lax.broadcasted_iota(jnp.int32, (BLK, BLK), 1)
    causal = ri >= ci
    tri = jnp.where(causal, 1.0, 0.0).astype(F32)
    lsc[...] = jnp.zeros((8, 256), F32)
    loaded("log")
    for b in range(4):
        lsc[b : b + 1, 0:128] = log_ref[2 * b : 2 * b + 1, :]
        lsc[b : b + 1, 128:256] = log_ref[2 * b + 1 : 2 * b + 2, :]
    logs = lsc[...]
    crow[...] = lax.dot_general(logs, tri, NT, precision=HIGH, preferred_element_type=F32)
    ccol[...] = lax.dot_general(tri, logs, NT, precision=HIGH, preferred_element_type=F32)
    loaded("k", "ti", "tb", "v")
    base = tb_ref[...]

    def turned(ref, b):
        ci_, si_ = ti_ref[0], ti_ref[1]
        cb_, sb_ = base[b : b + 1, :], base[4 + b : 5 + b, :]
        cos = cb_ * ci_ - sb_ * si_
        sin = sb_ * ci_ + cb_ * si_
        front = ref[b * BLK : (b + 1) * BLK, 0:128].astype(F32)
        second = ref[b * BLK : (b + 1) * BLK, 128:256].astype(F32)
        return front * cos - second * sin, front * sin + second * cos

    decay = jnp.ones((1, 1), F32)
    for b in range(4):
        front, second = turned(kv, b)
        front = (front * 0.0625).astype(BF16)
        second = (second * 0.0625).astype(BF16)
        kr[b, :, 0:128] = front
        kr[b, :, 128:256] = second
        total = crow[b : b + 1, 255:256]
        to_end = jnp.exp(total - ccol[:, b : b + 1])
        faded = jnp.concatenate([front, second], axis=1).astype(F32) * to_end
        state = lax.dot_general(
            faded.astype(BF16), vv[b * BLK : (b + 1) * BLK, :], TN, preferred_element_type=F32
        )
        step = jnp.exp(total)
        dpre[b] = jnp.broadcast_to(decay, (8, 128))
        decay = decay * step
        if b == 0:
            loc[b] = jnp.zeros((BLK, 512), F32)
            loc[b + 1] = state
        else:
            loc[b + 1] = step * loc[b] + state

    hi = decay.astype(BF16)
    mid = (decay - hi.astype(F32)).astype(BF16)
    low = (decay - hi.astype(F32) - mid.astype(F32)).astype(BF16)
    row = lax.broadcasted_iota(jnp.int32, (16, 128), 0)
    tag = jnp.where(
        row == 0,
        hi.astype(F32),
        jnp.where(row == 1, mid.astype(F32), jnp.where(row == 2, low.astype(F32), 0.0)),
    ).astype(BF16)
    for j in range(NSP):
        ssend[j, :, 0:512] = loc[4, j * 16 : (j + 1) * 16, :].astype(BF16)
        ssend[j, :, 512:640] = tag

    pl.semaphore_wait(barrier, NSP + 2)

    def scatter(i, carry):
        j, dev = sp_peer(i)
        remote(ssend.at[j], srecv.at[me], st_s.at[0], st_r.at[0], dev).start()
        return carry

    lax.fori_loop(1, NSP, scatter, 0)
    srecv[me] = ssend[me]

    pltpu.make_async_copy(ust, ust, in_sem.at[5]).wait()
    for n in range(11):
        tile = ust[n * 128 : (n + 1) * 128, :].astype(F32)
        wu[me, :, n * 128 : (n + 1) * 128] = tile.T.astype(BF16)
    u0()

    loaded("q")
    for b in range(4):
        front, second = turned(qv, b)
        qr = jnp.concatenate([front, second], axis=1).astype(BF16)
        column = ccol[:, b : b + 1]
        sq[b] = (qr.astype(F32) * jnp.exp(column)).astype(BF16)
        scores = lax.dot_general(qr, kr[b], NT, preferred_element_type=F32)
        gap = column - crow[b : b + 1, :]
        weight = jnp.where(causal, jnp.exp(jnp.where(causal, gap, 0.0)), 0.0)
        within[b] = jnp.dot(
            (scores * weight).astype(BF16),
            vv[b * BLK : (b + 1) * BLK, :],
            preferred_element_type=F32,
        )
    wd[FF:FFP, :] = jnp.zeros((FFP - FF, 2048), BF16)
    act0[:, :, FF:FFP] = jnp.zeros((4, 96, FFP - FF), BF16)
    act1[:, :, FF:FFP] = jnp.zeros((4, 160, FFP - FF), BF16)

    fifteen = slice(0, NSP - 1)
    scattered = remote(ssend.at[fifteen], srecv.at[fifteen], st_s.at[0], st_r.at[0], YR)
    returned = remote(rsend.at[fifteen], inc.at[fifteen], st_s.at[1], st_r.at[1], YR)
    scattered.wait_recv()
    acc = jnp.zeros((16, 512), F32)
    for d in range(NSP):
        rsend[d] = acc.astype(BF16)
        if d < NSP - 1:
            tags = srecv[d, :, 512:640].astype(F32)
            factor = tags[0:1, 0:1] + tags[1:2, 0:1] + tags[2:3, 0:1]
            acc = factor * acc + srecv[d, :, 0:512].astype(F32)
    inc[me] = rsend[me]

    def give_back(i, carry):
        j, dev = sp_peer(i)
        remote(rsend.at[j], inc.at[me], st_s.at[1], st_r.at[1], dev).start()
        return carry

    lax.fori_loop(1, NSP, give_back, 0)
    u0b()
    u1()

    returned.wait_recv()

    order = (xo, xr, xl, x)
    L, R = slice(0, 1024), slice(1024, 2048)

    class Scatter:
        def __init__(self, s, h):
            self.s, self.h = s, h
            self.lo, self.hi = ROWS[s][h]
            rows = slice(self.lo, self.hi)

            def across(n, src, dst, dev):
                return remote(src, dst, x_s.at[s, h], x_r.at[s, h, n], dev)

            self.a_out = across(0, cb.at[s, 0, rows, L], ra.at[s, rows], XR)
            self.b_out = across(1, cb.at[s, 0, rows, R], rb.at[s, rows], XL)
            self.r_late = across(2, cb.at[s, 1, rows, L], rl.at[s, rows, L], XR)
            self.r_soon = across(2, cb.at[s, 1, rows, R], rl.at[s, rows, R], XR)
            self.l_soon = across(2, cb.at[s, 2, rows, L], rr.at[s, rows, L], XL)
            self.l_late = across(2, cb.at[s, 2, rows, R], rr.at[s, rows, R], XL)
            self.into = across(2, cb.at[s, 0:2, rows], d2.at[s, 0:2, rows], XR)
            self.away = across(2, cb.at[s, 0:3, rows], d2.at[s, 0:3, rows], XR)

        def pair(self, j):
            s, h, rows = self.s, self.h, slice(self.lo, self.hi)
            return remote(
                part.at[s, j, 1 - c, rows], d2.at[s, j, rows], d2_s.at[s, h], d2_r.at[s, h, j], SIB
            )

        def merged(self, j, cols, extra=None):
            s = self.s

            def step(i, carry):
                r = pl.ds(pl.multiple_of(self.lo + i * 16, 16), 16)
                v = part[s, j, c, r, cols].astype(F32) + d2[s, j, r, cols].astype(F32)
                if extra is not None:
                    v = v + extra[s, r, :].astype(F32)
                cb[s, j, r, cols] = v.astype(BF16)
                return carry

            lax.fori_loop(0, (self.hi - self.lo) // 16, step, 0)

        def far(self):
            self.pair(0).wait_recv()
            self.merged(0, L)
            self.a_out.start()
            self.merged(0, R)
            self.b_out.start()

        def soon_right(self):
            self.pair(1).wait_recv()
            self.merged(1, R)
            self.r_soon.start()

        def soon_left(self):
            self.pair(2).wait_recv()
            self.merged(2, L)
            self.l_soon.start()

        def late(self):
            self.a_out.wait_recv()
            self.merged(1, L, ra)
            self.r_late.start()
            self.b_out.wait_recv()
            self.merged(2, R, rb)
            self.l_late.start()

        def finish(self):
            self.pair(3).wait_recv()
            self.into.wait_recv()

        def each(self, step):
            def run(i, carry):
                step(pl.ds(pl.multiple_of(self.lo + i * 16, 16), 16))
                return carry

            lax.fori_loop(0, (self.hi - self.lo) // 16, run, 0)

        def drain(self):
            s, h, rows = self.s, self.h, slice(self.lo, self.hi)
            remote(
                d2.at[s, :, rows], d2.at[s, :, rows], d2_s.at[s, h], d2_r.at[s, h, 0], SIB
            ).wait_send()
            self.away.wait_send()

    def summed(s, r):
        v = part[s, 3, c, r, :].astype(F32) + d2[s, 3, r, :].astype(F32)
        return v + rl[s, r, :].astype(F32) + rr[s, r, :].astype(F32)

    def normed(v, i):
        mean = jnp.mean(v, axis=-1, keepdims=True)
        v = v - mean
        var = jnp.mean(v * v, axis=-1, keepdims=True)
        return v * lax.rsqrt(var + EPS) * gain_ref[i : i + 1, :] + bias_ref[i : i + 1, :]

    loaded("g", "ow")

    def attend(j, b):
        rows = pl.ds(pl.multiple_of(b * BLK, BLK), BLK)
        state = dpre[b][0:1, 0:1] * inc[...].reshape(BLK, 512).astype(F32) + loc[b]
        mixed = within[b] + jnp.dot(sq[b], state.astype(BF16), preferred_element_type=F32)
        mean = jnp.mean(mixed, axis=-1, keepdims=True)
        mixed = mixed - mean
        var = jnp.mean(mixed * mixed, axis=-1, keepdims=True)
        mixed = mixed * lax.rsqrt(var + EPS)
        gate = gv[rows, :].astype(F32)
        gr[...] = (gate * jax.nn.sigmoid(gate) * mixed).astype(BF16)

        def tile(n, carry):
            cols = pl.ds(pl.multiple_of(n * 512, 512), 512)
            p = jnp.dot(gr[...], owv[:, cols], preferred_element_type=F32)
            part[0, j, :, :, cols] = p.astype(BF16).reshape(2, 128, 512)
            return carry

        lax.fori_loop(0, 4, tile, 0)

    A = [Scatter(0, 0), Scatter(0, 1)]
    attend(0, order[0])
    for h in A:
        h.pair(0).start()
    attend(1, order[1])
    for h in A:
        h.pair(1).start()
    for h in A:
        h.far()
    attend(2, order[2])
    for h in A:
        h.pair(2).start()
    for h in A:
        h.soon_right()
    attend(3, order[3])
    for h in A:
        h.pair(3).start()
    for h in A:
        h.soon_left()
    u2()
    u3(0)
    u3(1)
    for h in A:
        h.late()
    u3(2)
    u3(3)
    loaded("dw")
    n0()
    n0b()
    loaded("res", "gain", "bias")

    def first_norm(r):
        v = ALPHA * rv[r, :].astype(F32) + summed(0, r)
        xb[t, r, :] = normed(v, 0).astype(BF16)

    tl, tr, to = xl * 2 + c, xr * 2 + c, xo * 2 + c
    W = slice(0, 2048)

    def ag(h, n, owner, cols, dev):
        lo, hi = ROWS[0][h]
        p = xb.at[owner, lo:hi, cols]
        return remote(p, p, ag_s.at[h], ag_r.at[h, n], dev)

    def go(h, n, owner, cols, dev):
        ag(h, n, owner, cols, dev).start()

    def several(h, n, owners):
        lo, hi = ROWS[0][h]
        p = xb.at[0:owners, lo:hi]
        return remote(p, p, ag_s.at[h], ag_r.at[h, n], SIB)

    def arrived(h, n, owner, cols):
        ag(h, n, owner, cols, SIB).wait_recv()

    def own_rows(h):
        go(h, 1, t, L, XR)
        go(h, 3, t, R, XL)
        go(h, 0, t, W, SIB)
        go(h, 2, t, R, XR)
        go(h, 4, t, L, XL)

    def pass_on(h):
        arrived(h, 1, tl, L)
        go(h, 5, tl, L, XR)
        arrived(h, 3, tr, R)
        go(h, 6, tr, R, XL)
        go(h, 7, tl, L, SIB)
        go(h, 7, tr, R, SIB)

    def pass_second(h):
        arrived(h, 2, tl, R)
        go(h, 7, tl, R, SIB)
        arrived(h, 4, tr, L)
        go(h, 7, tr, L, SIB)

    def near_ready(h):
        several(h, 7, 2).wait_recv()

    def pass_far(h):
        arrived(h, 5, to, L)
        go(h, 8, to, L, SIB)
        arrived(h, 6, to, R)
        go(h, 8, to, R, SIB)

    def far_ready(h):
        several(h, 8, 1).wait_recv()

    def up(h, *chips):
        lo, hi = ROWS[0][h]

        def cols_of(cols, width):
            lhs = [xb[pl.ds(2 * b, 2), lo:hi].reshape(128, 2048) for b in chips]
            lhs = lhs[0] if len(lhs) == 1 else jnp.concatenate(lhs, axis=0)
            w = wu[:, :, cols].reshape(2048, width)
            out = jnp.dot(lhs, w, preferred_element_type=F32).astype(BF16)
            for i, b in enumerate(chips):
                for d in range(2):
                    at_row = pl.multiple_of(16 + (2 * b + d) * 128 + lo, 16)
                    ub[pl.ds(at_row, 64), cols] = out[(2 * i + d) * 64 : (2 * i + d + 1) * 64]

        def tile(n, carry):
            cols_of(pl.ds(pl.multiple_of(n * 256, 256), 256), 256)
            return carry

        lax.fori_loop(0, 5, tile, 0)
        cols_of(slice(1280, 1408), 128)

    def halo_copy():
        nxt = lax.rem(me + 1, NSP)
        dev = {"z": lax.div(nxt, 4), "y": lax.rem(nxt, 4)}
        return remote(ub.at[1024:1040, :], halo, h_s.at[0], h_r.at[0], dev)

    def send_halo(when):
        @pl.when(jnp.logical_and(when, me < NSP - 1))
        def _():
            halo_copy().start()

    @pl.when(me == 0)
    def _():
        ub[0:16, :] = jnp.zeros((16, 1408), BF16)

    def conv(g, b):
        lo, hi = ROWS[1][g]
        n_rows = hi - lo
        act = (act0, act1)[g]

        def three(block, half, lanes):
            v = shift_ref[half : half + 1, lanes] + block[14 : 14 + n_rows] * taps_ref[0, half : half + 1, lanes]
            v = v + block[15 : 15 + n_rows] * taps_ref[1, half : half + 1, lanes]
            return v + block[16 : 16 + n_rows] * taps_ref[2, half : half + 1, lanes]

        def device(d, carry):
            around = pl.ds(pl.multiple_of((2 * b + d) * 128 + lo, 16), n_rows + 16)
            rows = pl.ds(pl.multiple_of(d * n_rows, 16), n_rows)
            for n in range(6):
                if n < 5:
                    lanes = slice(n * 128, (n + 1) * 128)
                    gate = ub[around, lanes].astype(F32)
                    value = ub[around, 640 + n * 128 : 640 + (n + 1) * 128].astype(F32)
                else:
                    lanes = slice(640, FF)
                    both = ub[around, 1280:1408].astype(F32)
                    gate, value = both[:, 0:64], pltpu.roll(both, 64, 1)[:, 0:64]
                a = jax.nn.gelu(three(gate, 0, lanes)) * three(value, 1, lanes)
                act[b, rows, lanes] = a.astype(BF16)
            return carry

        lax.fori_loop(0, 2, device, 0)

    def down(g, j, b):
        lo, hi = ROWS[1][g]
        act = (act0, act1)[g]

        def tile(n, carry):
            cols = pl.ds(pl.multiple_of(n * 512, 512), 512)
            p = jnp.dot(act[b], wd[:, cols], preferred_element_type=F32)
            part[1, j, :, lo:hi, cols] = p.astype(BF16).reshape(2, hi - lo, 512)
            return carry

        lax.fori_loop(0, 4, tile, 0)

    B = [Scatter(1, 0), Scatter(1, 1)]
    A[0].finish()
    A[0].each(first_norm)
    own_rows(0)
    A[1].finish()
    A[1].each(first_norm)
    u4()
    n1()
    loaded("taps", "shift")
    arrived(0, 0, t + 1 - 2 * c, W)
    up(0, x)
    send_halo(x == 3)
    pass_on(0)
    own_rows(1)
    pass_second(0)
    arrived(1, 0, t + 1 - 2 * c, W)
    up(1, x)
    n2()
    n3(0)
    n3(1)
    n3(2)
    near_ready(0)
    up(0, xr, xl)
    send_halo(jnp.logical_or(xr == 3, xl == 3))
    pass_far(0)
    conv(0, x)
    conv(0, xr)
    conv(0, xl)
    pass_on(1)
    n3(3)
    far_ready(0)
    up(0, xo)
    send_halo(xo == 3)
    conv(0, xo)
    n4()
    down(0, 0, xo)
    B[0].pair(0).start()
    pass_second(1)
    down(0, 1, xr)
    B[0].pair(1).start()
    B[0].far()
    down(0, 2, xl)
    B[0].pair(2).start()
    B[0].soon_right()
    pass_far(1)
    near_ready(1)
    up(1, xr, xl)
    B[0].soon_left()
    B[0].late()
    far_ready(1)
    up(1, xo)

    @pl.when(me > 0)
    def _():
        halo_copy().wait_recv()
        ub[0:16, :] = halo[...]

    conv(1, xo)
    down(1, 0, xo)
    B[1].pair(0).start()
    conv(1, xr)
    down(1, 1, xr)
    B[1].pair(1).start()
    B[1].far()
    conv(1, xl)
    down(1, 2, xl)
    B[1].pair(2).start()
    B[1].soon_right()
    conv(1, x)
    down(1, 3, x)
    B[1].pair(3).start()
    B[1].soon_left()
    B[1].late()
    down(0, 3, x)
    B[0].pair(3).start()

    def last_norm(r):
        v = ALPHA * xb[t, r, :].astype(F32) + summed(1, r)
        ov[r, :] = normed(v, 1).astype(BF16)

    outs = []
    for g in range(2):
        B[g].finish()
        B[g].each(last_norm)
        lo, hi = ROWS[1][g]
        outs.append(pltpu.make_async_copy(ov.at[lo:hi], o_ref.at[lo:hi], out_sem.at[g]))
        outs[g].start()

    scattered.wait_send()
    returned.wait_send()
    udrain()
    ndrain()
    for op in A + B:
        op.drain()
    for h in range(2):
        several(h, 0, 7).wait_send()

    @pl.when(me < NSP - 1)
    def _():
        halo_copy().wait_send()

    for op in outs:
        op.wait()


def shards(q, k, v, g, logd, res, ow, gain, bias, ug, uv, cw, cbias, dw):
    ti, tb = position_tables()
    dma = pltpu.SemaphoreType.DMA
    hb = pl.BlockSpec(memory_space=pl.ANY)
    return pl.pallas_call(
        body,
        out_shape=jax.ShapeDtypeStruct((128, 2048), BF16),
        in_specs=[hb] * 16,
        out_specs=hb,
        scratch_shapes=[
            pltpu.VMEM((1024, 256), BF16),
            pltpu.VMEM((1024, 256), BF16),
            pltpu.VMEM((1024, 512), BF16),
            pltpu.VMEM((1024, 512), BF16),
            pltpu.VMEM((8, 128), F32),
            pltpu.VMEM((128, 2048), BF16),
            pltpu.VMEM((512, 2048), BF16),
            pltpu.VMEM((2, 2048), F32),
            pltpu.VMEM((2, 2048), F32),
            pltpu.VMEM((1408, 128), BF16),
            pltpu.VMEM((3, 2, FF), F32),
            pltpu.VMEM((2, FF), F32),
            pltpu.VMEM((2, BLK, 128), F32),
            pltpu.VMEM((8, 128), F32),
            pltpu.VMEM((NSP, 128, 1408), BF16),
            pltpu.VMEM((FFP, 2048), BF16),
            pltpu.VMEM((8, 256), F32),
            pltpu.VMEM((8, 256), F32),
            pltpu.VMEM((256, 8), F32),
            pltpu.VMEM((4, 8, 128), F32),
            pltpu.VMEM((4, 256, 256), BF16),
            pltpu.VMEM((4, 256, 256), BF16),
            pltpu.VMEM((5, 256, 512), F32),
            pltpu.VMEM((4, 256, 512), F32),
            pltpu.VMEM((256, 512), BF16),
            pltpu.VMEM((NSP, 16, 640), BF16),
            pltpu.VMEM((NSP, 16, 640), BF16),
            pltpu.VMEM((NSP, 16, 512), BF16),
            pltpu.VMEM((NSP, 16, 512), BF16),
            pltpu.VMEM((2, 4, 2, 128, 2048), BF16),
            pltpu.VMEM((2, 4, 128, 2048), BF16),
            pltpu.VMEM((2, 3, 128, 2048), BF16),
            pltpu.VMEM((2, 128, 1024), BF16),
            pltpu.VMEM((2, 128, 1024), BF16),
            pltpu.VMEM((2, 128, 2048), BF16),
            pltpu.VMEM((2, 128, 2048), BF16),
            pltpu.VMEM((8, 128, 2048), BF16),
            pltpu.VMEM((1040, 1408), BF16),
            pltpu.VMEM((4, 96, FFP), BF16),
            pltpu.VMEM((4, 160, FFP), BF16),
            pltpu.VMEM((16, 1408), BF16),
            pltpu.VMEM((128, 2048), BF16),
            dma((18,)),
            dma((2,)),
            dma((2,)),
            dma((2,)),
            dma((2, 7)),
            dma((2, 2)),
            dma((2, 2, 4)),
            dma((2, 2)),
            dma((2, 2, 3)),
            dma((2,)),
            dma((2, 9)),
            dma((1,)),
            dma((1,)),
            dma((2,)),
        ],
        compiler_params=pltpu.CompilerParams(
            collective_id=0, has_side_effects=True, vmem_limit_bytes=62 * 1024 * 1024
        ),
        name="layer",
    )(
        q, k, v, g, logd.reshape(8, 128), res, ow, gain, bias, ug.T, uv.T,
        cw.transpose(1, 0, 2), cbias, dw, ti, tb,
    )


def solution(mesh):
    torus = Mesh(mesh.devices.reshape(4, 4, 4, 2), ("z", "y", "x", "c"))
    sp, tp = ("z", "y"), ("x", "c")
    return jax.shard_map(
        shards,
        mesh=torus,
        in_specs=(
            P(sp, tp),
            P(sp, tp),
            P(sp, tp),
            P(sp, tp),
            P(sp, tp),
            P(sp, None),
            P(tp, None),
            P(),
            P(),
            P(sp, tp),
            P(sp, tp),
            P(None, None, tp),
            P(None, tp),
            P(tp, sp),
        ),
        out_specs=P(sp + tp, None),
        check_vma=False,
    )
```

time: 103 us -> 92.8 us (0.901)
  Pallas kernels: 101 us -> 90.8 us
    pallas_call x1, Pallas kernels: 101 us -> 90.8 us  [shards(): pl.pallas_call(body, out_shape=jax.ShapeDtypeStruct((128, 2048), BF16), i...]
where the time goes in v3:
time: 92.8 us; the launch traced here: 92.6 us
  Pallas kernels  90.8 us (98%)
  local copies, waits for them, and re-layouts  1.88 us (2%)
    pallas_call x1, Pallas kernels, shards(): pl.pallas_call(body, out_shape=jax.ShapeDtypeStruct((128, 2048), BF16), i...  90.8 us
    unnamed x1, local copies, waits for them, and re-layouts  1.88 us

profile of v3, /device:TPU:1, one launch (start us, length us, event | category | flops | bytes accessed | tf_op | source)
XLA Modules:
  0.0 92.6 jit_solution(17068001988466725237)
XLA Ops:
  0.0 90.8 %layer.1 = bf16[128,2048]{1,0:T(8,128)(2,1)} custom-call(bf16[1024,256]{1,0:T(8,128)(2,1)} %q_h.1, bf16[1024,256]{1,0:T(8,128)(2,1)} %k_h.1, bf16[1024,512]{1,0:T(8,128)(2,1)} %v_h.1, bf16[1024,512]{1,0:T(8,128)(2,1)} %g_h.1, f32[8,128]{1,0:T(8,128)} %bitcast.7, bf16[1024,2048]{1,0:T(8,128)(2,1)} %res_h.1, bf16[512,2048]{1,0:T(8,128)(2,1)} %ow_h.1, ...), custom_call_target="tpu_custom_call" | custom-call | tf_op jit(solution)/shard_map/layer/pallas_call | solution.py:687
  90.8 1.9 %copy.18 = bf16[128,2048]{1,0:T(8,128)(2,1)} copy(bf16[128,2048]{1,0:T(8,128)(2,1)} %layer.1) | data formatting | bytes 1048576

commit v4 on v3

--- a/solution.py
+++ b/solution.py
@@ -19,7 +19,7 @@
 BLK = 256
 FF = 704
 FFP = 768
-ROWS = (((64, 128), (0, 64)), ((80, 128), (0, 80)))
+ROWS = (((48, 128), (0, 48)), ((64, 128), (0, 64)))
 NT = (((1,), (1,)), ((), ()))
 TN = (((0,), (0,)), ((), ()))
 
@@ -273,8 +273,8 @@
             preferred_element_type=F32,
         )
     wd[FF:FFP, :] = jnp.zeros((FFP - FF, 2048), BF16)
-    act0[:, :, FF:FFP] = jnp.zeros((4, 96, FFP - FF), BF16)
-    act1[:, :, FF:FFP] = jnp.zeros((4, 160, FFP - FF), BF16)
+    act0[:, :, FF:FFP] = jnp.zeros((4, 128, FFP - FF), BF16)
+    act1[:, :, FF:FFP] = jnp.zeros((4, 128, FFP - FF), BF16)
 
     fifteen = slice(0, NSP - 1)
     scattered = remote(ssend.at[fifteen], srecv.at[fifteen], st_s.at[0], st_r.at[0], YR)
@@ -330,15 +330,14 @@
         def merged(self, j, cols, extra=None):
             s = self.s
 
-            def step(i, carry):
-                r = pl.ds(pl.multiple_of(self.lo + i * 16, 16), 16)
+            for r in self.steps():
                 v = part[s, j, c, r, cols].astype(F32) + d2[s, j, r, cols].astype(F32)
                 if extra is not None:
                     v = v + extra[s, r, :].astype(F32)
                 cb[s, j, r, cols] = v.astype(BF16)
-                return carry
-
-            lax.fori_loop(0, (self.hi - self.lo) // 16, step, 0)
+
+        def steps(self):
+            return [slice(r, min(r + 32, self.hi)) for r in range(self.lo, self.hi, 32)]
 
         def far(self):
             self.pair(0).wait_recv()
@@ -370,11 +369,8 @@
             self.into.wait_recv()
 
         def each(self, step):
-            def run(i, carry):
-                step(pl.ds(pl.multiple_of(self.lo + i * 16, 16), 16))
-                return carry
-
-            lax.fori_loop(0, (self.hi - self.lo) // 16, run, 0)
+            for r in self.steps():
+                step(r)
 
         def drain(self):
             s, h, rows = self.s, self.h, slice(self.lo, self.hi)
@@ -395,7 +391,7 @@
 
     loaded("g", "ow")
 
-    def attend(j, b):
+    def mix(b):
         rows = pl.ds(pl.multiple_of(b * BLK, BLK), BLK)
         state = dpre[b][0:1, 0:1] * inc[...].reshape(BLK, 512).astype(F32) + loc[b]
         mixed = within[b] + jnp.dot(sq[b], state.astype(BF16), preferred_element_type=F32)
@@ -404,41 +400,47 @@
         var = jnp.mean(mixed * mixed, axis=-1, keepdims=True)
         mixed = mixed * lax.rsqrt(var + EPS)
         gate = gv[rows, :].astype(F32)
-        gr[...] = (gate * jax.nn.sigmoid(gate) * mixed).astype(BF16)
-
+        gr[...] = (gate * jax.nn.sigmoid(gate) * mixed).astype(BF16).reshape(2, 128, 512)
+
+    def project(j, lo=0, hi=128):
         def tile(n, carry):
             cols = pl.ds(pl.multiple_of(n * 512, 512), 512)
-            p = jnp.dot(gr[...], owv[:, cols], preferred_element_type=F32)
-            part[0, j, :, :, cols] = p.astype(BF16).reshape(2, 128, 512)
+            lhs = gr[:, lo:hi].reshape(2 * (hi - lo), 512)
+            p = jnp.dot(lhs, owv[:, cols], preferred_element_type=F32)
+            part[0, j, :, lo:hi, cols] = p.astype(BF16).reshape(2, hi - lo, 512)
             return carry
 
         lax.fori_loop(0, 4, tile, 0)
 
     A = [Scatter(0, 0), Scatter(0, 1)]
-    attend(0, order[0])
+    mix(order[0])
     for h in A:
+        project(0, h.lo, h.hi)
         h.pair(0).start()
-    attend(1, order[1])
+    mix(order[1])
+    A[0].far()
+    project(1)
     for h in A:
         h.pair(1).start()
-    for h in A:
-        h.far()
-    attend(2, order[2])
+    mix(order[2])
+    project(2)
     for h in A:
         h.pair(2).start()
-    for h in A:
-        h.soon_right()
-    attend(3, order[3])
+    A[0].soon_right()
+    A[1].far()
+    mix(order[3])
+    project(3)
     for h in A:
         h.pair(3).start()
-    for h in A:
-        h.soon_left()
+    A[0].soon_left()
+    A[0].late()
+    A[1].soon_right()
+    A[1].soon_left()
     u2()
     u3(0)
     u3(1)
-    for h in A:
-        h.late()
     u3(2)
+    A[1].late()
     u3(3)
     loaded("dw")
     n0()
@@ -471,7 +473,8 @@
     def own_rows(h):
         go(h, 1, t, L, XR)
         go(h, 3, t, R, XL)
-        go(h, 0, t, W, SIB)
+        if h == 0:
+            go(h, 0, t, W, SIB)
         go(h, 2, t, R, XR)
         go(h, 4, t, L, XL)
 
@@ -503,16 +506,17 @@
 
     def up(h, *chips):
         lo, hi = ROWS[0][h]
+        rows = hi - lo
 
         def cols_of(cols, width):
-            lhs = [xb[pl.ds(2 * b, 2), lo:hi].reshape(128, 2048) for b in chips]
+            lhs = [xb[pl.ds(2 * b, 2), lo:hi].reshape(2 * rows, 2048) for b in chips]
             lhs = lhs[0] if len(lhs) == 1 else jnp.concatenate(lhs, axis=0)
             w = wu[:, :, cols].reshape(2048, width)
             out = jnp.dot(lhs, w, preferred_element_type=F32).astype(BF16)
             for i, b in enumerate(chips):
                 for d in range(2):
                     at_row = pl.multiple_of(16 + (2 * b + d) * 128 + lo, 16)
-                    ub[pl.ds(at_row, 64), cols] = out[(2 * i + d) * 64 : (2 * i + d + 1) * 64]
+                    ub[pl.ds(at_row, rows), cols] = out[(2 * i + d) * rows : (2 * i + d + 1) * rows]
 
         def tile(n, carry):
             cols_of(pl.ds(pl.multiple_of(n * 256, 256), 256), 256)
@@ -563,14 +567,18 @@
 
         lax.fori_loop(0, 2, device, 0)
 
-    def down(g, j, b):
+    def down(g, js, chips):
         lo, hi = ROWS[1][g]
         act = (act0, act1)[g]
 
         def tile(n, carry):
             cols = pl.ds(pl.multiple_of(n * 512, 512), 512)
-            p = jnp.dot(act[b], wd[:, cols], preferred_element_type=F32)
-            part[1, j, :, lo:hi, cols] = p.astype(BF16).reshape(2, hi - lo, 512)
+            lhs = [act[b] for b in chips]
+            lhs = lhs[0] if len(lhs) == 1 else jnp.concatenate(lhs, axis=0)
+            p = jnp.dot(lhs, wd[:, cols], preferred_element_type=F32).astype(BF16)
+            p = p.reshape(len(js), 2, hi - lo, 512)
+            for i, j in enumerate(js):
+                part[1, j, :, lo:hi, cols] = p[i]
             return carry
 
         lax.fori_loop(0, 4, tile, 0)
@@ -581,51 +589,51 @@
     own_rows(0)
     A[1].finish()
     A[1].each(first_norm)
+    go(1, 0, t, W, SIB)
     u4()
-    n1()
     loaded("taps", "shift")
     arrived(0, 0, t + 1 - 2 * c, W)
     up(0, x)
     send_halo(x == 3)
     pass_on(0)
     own_rows(1)
+    n1()
+    conv(0, x)
     pass_second(0)
     arrived(1, 0, t + 1 - 2 * c, W)
     up(1, x)
+    near_ready(0)
     n2()
     n3(0)
-    n3(1)
-    n3(2)
-    near_ready(0)
     up(0, xr, xl)
     send_halo(jnp.logical_or(xr == 3, xl == 3))
     pass_far(0)
-    conv(0, x)
+    n3(1)
     conv(0, xr)
     conv(0, xl)
     pass_on(1)
+    n3(2)
     n3(3)
     far_ready(0)
     up(0, xo)
     send_halo(xo == 3)
+    pass_second(1)
     conv(0, xo)
     n4()
-    down(0, 0, xo)
+    down(0, (0,), (xo,))
     B[0].pair(0).start()
-    pass_second(1)
-    down(0, 1, xr)
+    down(0, (1, 2), (xr, xl))
     B[0].pair(1).start()
+    B[0].pair(2).start()
+    pass_far(1)
     B[0].far()
-    down(0, 2, xl)
-    B[0].pair(2).start()
+    down(0, (3,), (x,))
+    B[0].pair(3).start()
     B[0].soon_right()
-    pass_far(1)
+    B[0].soon_left()
     near_ready(1)
-    up(1, xr, xl)
-    B[0].soon_left()
-    B[0].late()
     far_ready(1)
-    up(1, xo)
+    up(1, xo, xr, xl)
 
     @pl.when(me > 0)
     def _():
@@ -633,23 +641,21 @@
         ub[0:16, :] = halo[...]
 
     conv(1, xo)
-    down(1, 0, xo)
+    down(1, (0,), (xo,))
     B[1].pair(0).start()
+    B[0].late()
     conv(1, xr)
-    down(1, 1, xr)
+    down(1, (1,), (xr,))
     B[1].pair(1).start()
     B[1].far()
     conv(1, xl)
-    down(1, 2, xl)
+    down(1, (2,), (xl,))
     B[1].pair(2).start()
     B[1].soon_right()
     conv(1, x)
-    down(1, 3, x)
+    down(1, (3,), (x,))
     B[1].pair(3).start()
     B[1].soon_left()
-    B[1].late()
-    down(0, 3, x)
-    B[0].pair(3).start()
 
     def last_norm(r):
         v = ALPHA * xb[t, r, :].astype(F32) + summed(1, r)
@@ -657,6 +663,8 @@
 
     outs = []
     for g in range(2):
+        if g == 1:
+            B[g].late()
         B[g].finish()
         B[g].each(last_norm)
         lo, hi = ROWS[1][g]
@@ -714,7 +722,7 @@
             pltpu.VMEM((4, 256, 256), BF16),
             pltpu.VMEM((5, 256, 512), F32),
             pltpu.VMEM((4, 256, 512), F32),
-            pltpu.VMEM((256, 512), BF16),
+            pltpu.VMEM((2, 128, 512), BF16),
             pltpu.VMEM((NSP, 16, 640), BF16),
             pltpu.VMEM((NSP, 16, 640), BF16),
             pltpu.VMEM((NSP, 16, 512), BF16),
@@ -728,8 +736,8 @@
             pltpu.VMEM((2, 128, 2048), BF16),
             pltpu.VMEM((8, 128, 2048), BF16),
             pltpu.VMEM((1040, 1408), BF16),
-            pltpu.VMEM((4, 96, FFP), BF16),
-            pltpu.VMEM((4, 160, FFP), BF16),
+            pltpu.VMEM((4, 128, FFP), BF16),
+            pltpu.VMEM((4, 128, FFP), BF16),
             pltpu.VMEM((16, 1408), BF16),
             pltpu.VMEM((128, 2048), BF16),
             dma((18,)),

time: 92.8 us -> 89.7 us (0.967)
  Pallas kernels: 90.8 us -> 87.6 us
    pallas_call x1, Pallas kernels: 90.8 us -> 87.6 us  [shards(): pl.pallas_call(body, out_shape=jax.ShapeDtypeStruct((128, 2048), BF16), i...]
where the time goes in v4:
time: 89.7 us; the launch traced here: 89.5 us
  Pallas kernels  87.6 us (98%)
  local copies, waits for them, and re-layouts  1.88 us (2%)
    pallas_call x1, Pallas kernels, shards(): pl.pallas_call(body, out_shape=jax.ShapeDtypeStruct((128, 2048), BF16), i...  87.6 us
    unnamed x1, local copies, waits for them, and re-layouts  1.88 us

profile of v4, /device:TPU:1, one launch (start us, length us, event | category | flops | bytes accessed | tf_op | source)
XLA Modules:
  0.0 89.5 jit_solution(852203537720589169)
XLA Ops:
  0.0 87.6 %layer.1 = bf16[128,2048]{1,0:T(8,128)(2,1)} custom-call(bf16[1024,256]{1,0:T(8,128)(2,1)} %q_h.1, bf16[1024,256]{1,0:T(8,128)(2,1)} %k_h.1, bf16[1024,512]{1,0:T(8,128)(2,1)} %v_h.1, bf16[1024,512]{1,0:T(8,128)(2,1)} %g_h.1, f32[8,128]{1,0:T(8,128)} %bitcast.7, bf16[1024,2048]{1,0:T(8,128)(2,1)} %res_h.1, bf16[512,2048]{1,0:T(8,128)(2,1)} %ow_h.1, ...), custom_call_target="tpu_custom_call" | custom-call | tf_op jit(solution)/shard_map/layer/pallas_call | solution.py:695
  87.6 1.9 %copy.18 = bf16[128,2048]{1,0:T(8,128)(2,1)} copy(bf16[128,2048]{1,0:T(8,128)(2,1)} %layer.1) | data formatting | bytes 1048576

commit v5 on v4

--- a/solution.py
+++ b/solution.py
@@ -440,11 +440,11 @@
     u3(0)
     u3(1)
     u3(2)
-    A[1].late()
-    u3(3)
     loaded("dw")
     n0()
     n0b()
+    A[1].late()
+    u3(3)
     loaded("res", "gain", "bias")
 
     def first_norm(r):
@@ -504,19 +504,22 @@
     def far_ready(h):
         several(h, 8, 1).wait_recv()
 
-    def up(h, *chips):
-        lo, hi = ROWS[0][h]
-        rows = hi - lo
-
+    def up(*items):
         def cols_of(cols, width):
-            lhs = [xb[pl.ds(2 * b, 2), lo:hi].reshape(2 * rows, 2048) for b in chips]
+            lhs = []
+            for h, b in items:
+                lo, hi = ROWS[0][h]
+                lhs.append(xb[pl.ds(2 * b, 2), lo:hi].reshape(2 * (hi - lo), 2048))
             lhs = lhs[0] if len(lhs) == 1 else jnp.concatenate(lhs, axis=0)
             w = wu[:, :, cols].reshape(2048, width)
             out = jnp.dot(lhs, w, preferred_element_type=F32).astype(BF16)
-            for i, b in enumerate(chips):
+            k = 0
+            for h, b in items:
+                lo, hi = ROWS[0][h]
                 for d in range(2):
                     at_row = pl.multiple_of(16 + (2 * b + d) * 128 + lo, 16)
-                    ub[pl.ds(at_row, rows), cols] = out[(2 * i + d) * rows : (2 * i + d + 1) * rows]
+                    ub[pl.ds(at_row, hi - lo), cols] = out[k : k + hi - lo]
+                    k += hi - lo
 
         def tile(n, carry):
             cols_of(pl.ds(pl.multiple_of(n * 256, 256), 256), 256)
@@ -590,32 +593,31 @@
     A[1].finish()
     A[1].each(first_norm)
     go(1, 0, t, W, SIB)
+    n1()
+    pass_on(0)
+    own_rows(1)
     u4()
     loaded("taps", "shift")
     arrived(0, 0, t + 1 - 2 * c, W)
-    up(0, x)
+    arrived(1, 0, t + 1 - 2 * c, W)
+    up((0, x), (1, x))
     send_halo(x == 3)
-    pass_on(0)
-    own_rows(1)
-    n1()
-    conv(0, x)
     pass_second(0)
-    arrived(1, 0, t + 1 - 2 * c, W)
-    up(1, x)
-    near_ready(0)
     n2()
     n3(0)
-    up(0, xr, xl)
+    conv(0, x)
+    near_ready(0)
+    n3(1)
+    up((0, xr), (0, xl))
     send_halo(jnp.logical_or(xr == 3, xl == 3))
     pass_far(0)
-    n3(1)
+    n3(2)
     conv(0, xr)
     conv(0, xl)
     pass_on(1)
-    n3(2)
     n3(3)
     far_ready(0)
-    up(0, xo)
+    up((0, xo))
     send_halo(xo == 3)
     pass_second(1)
     conv(0, xo)
@@ -633,7 +635,7 @@
     B[0].soon_left()
     near_ready(1)
     far_ready(1)
-    up(1, xo, xr, xl)
+    up((1, xo), (1, xr), (1, xl))
 
     @pl.when(me > 0)
     def _():

time: 89.7 us -> 88.9 us (level)
  no operation moved by 1% of the time
where the time goes in v5:
time: 88.9 us; the launch traced here: 88.7 us
  Pallas kernels  86.8 us (98%)
  local copies, waits for them, and re-layouts  1.88 us (2%)
    pallas_call x1, Pallas kernels, shards(): pl.pallas_call(body, out_shape=jax.ShapeDtypeStruct((128, 2048), BF16), i...  86.8 us
    unnamed x1, local copies, waits for them, and re-layouts  1.88 us

profile of v5, /device:TPU:1, one launch (start us, length us, event | category | flops | bytes accessed | tf_op | source)
XLA Modules:
  0.0 88.7 jit_solution(581953441366877750)
XLA Ops:
  0.0 86.8 %layer.1 = bf16[128,2048]{1,0:T(8,128)(2,1)} custom-call(bf16[1024,256]{1,0:T(8,128)(2,1)} %q_h.1, bf16[1024,256]{1,0:T(8,128)(2,1)} %k_h.1, bf16[1024,512]{1,0:T(8,128)(2,1)} %v_h.1, bf16[1024,512]{1,0:T(8,128)(2,1)} %g_h.1, f32[8,128]{1,0:T(8,128)} %bitcast.7, bf16[1024,2048]{1,0:T(8,128)(2,1)} %res_h.1, bf16[512,2048]{1,0:T(8,128)(2,1)} %ow_h.1, ...), custom_call_target="tpu_custom_call" | custom-call | tf_op jit(solution)/shard_map/layer/pallas_call | solution.py:697
  86.9 1.9 %copy.18 = bf16[128,2048]{1,0:T(8,128)(2,1)} copy(bf16[128,2048]{1,0:T(8,128)(2,1)} %layer.1) | data formatting | bytes 1048576

commit v6 on v5

--- a/solution.py
+++ b/solution.py
@@ -647,9 +647,9 @@
     B[1].pair(0).start()
     B[0].late()
     conv(1, xr)
+    B[1].far()
     down(1, (1,), (xr,))
     B[1].pair(1).start()
-    B[1].far()
     conv(1, xl)
     down(1, (2,), (xl,))
     B[1].pair(2).start()
@@ -659,19 +659,19 @@
     B[1].pair(3).start()
     B[1].soon_left()
 
+    outs = []
+
     def last_norm(r):
         v = ALPHA * xb[t, r, :].astype(F32) + summed(1, r)
         ov[r, :] = normed(v, 1).astype(BF16)
-
-    outs = []
+        outs.append(pltpu.make_async_copy(ov.at[r], o_ref.at[r], out_sem.at[len(outs)]))
+        outs[-1].start()
+
     for g in range(2):
         if g == 1:
             B[g].late()
         B[g].finish()
         B[g].each(last_norm)
-        lo, hi = ROWS[1][g]
-        outs.append(pltpu.make_async_copy(ov.at[lo:hi], o_ref.at[lo:hi], out_sem.at[g]))
-        outs[g].start()
 
     scattered.wait_send()
     returned.wait_send()
@@ -755,7 +755,7 @@
             dma((2, 9)),
             dma((1,)),
             dma((1,)),
-            dma((2,)),
+            dma((4,)),
         ],
         compiler_params=pltpu.CompilerParams(
             collective_id=0, has_side_effects=True, vmem_limit_bytes=62 * 1024 * 1024

time: 88.9 us -> 88.9 us (level)
  no operation moved by 1% of the time
where the time goes in v6:
time: 88.9 us; the launch traced here: 88.7 us
  Pallas kernels  86.8 us (98%)
  local copies, waits for them, and re-layouts  1.88 us (2%)
    pallas_call x1, Pallas kernels, shards(): pl.pallas_call(body, out_shape=jax.ShapeDtypeStruct((128, 2048), BF16), i...  86.8 us
    unnamed x1, local copies, waits for them, and re-layouts  1.88 us

profile of v6, /device:TPU:1, one launch (start us, length us, event | category | flops | bytes accessed | tf_op | source)
XLA Modules:
  0.0 88.7 jit_solution(10094384465724953988)
XLA Ops:
  0.0 86.8 %layer.1 = bf16[128,2048]{1,0:T(8,128)(2,1)} custom-call(bf16[1024,256]{1,0:T(8,128)(2,1)} %q_h.1, bf16[1024,256]{1,0:T(8,128)(2,1)} %k_h.1, bf16[1024,512]{1,0:T(8,128)(2,1)} %v_h.1, bf16[1024,512]{1,0:T(8,128)(2,1)} %g_h.1, f32[8,128]{1,0:T(8,128)} %bitcast.7, bf16[1024,2048]{1,0:T(8,128)(2,1)} %res_h.1, bf16[512,2048]{1,0:T(8,128)(2,1)} %ow_h.1, ...), custom_call_target="tpu_custom_call" | custom-call | tf_op jit(solution)/shard_map/layer/pallas_call | solution.py:697
  86.8 1.9 %copy.18 = bf16[128,2048]{1,0:T(8,128)(2,1)} copy(bf16[128,2048]{1,0:T(8,128)(2,1)} %layer.1) | data formatting | bytes 1048576
